TPU v7x, 32 devices: a whole 2x2x4 slice. The times are simulated.
32 devices in a mesh: sp: 4 (over z), fs: 4 (over y, x), tp: 2 (over core).
Axes of the slice: x: 2, y: 2, z: 4, core: 2. Of those that a mesh axis runs over, the one named last changes fastest.
Arguments:
- tokens: bfloat16 [4, 1024, 2048], P('fs', 'sp', 'tp'), may hold values from -6 to 6
- norm_gain: float32 [2048], replicated, may hold values from 0.1 to 1.9
- query_weight: bfloat16 [2048, 1024], P('fs', 'tp'), may hold values from -1 to 1
- key_weight: bfloat16 [2048, 1024], P('fs', 'tp'), may hold values from -4 to 4
- value_weight: bfloat16 [2048, 1024], P('fs', 'tp'), may hold values from -0.125 to 0.125
- state_query: bfloat16 [2048, 1024], P('fs', 'tp'), may hold values from -0.125 to 0.125
- state_key: bfloat16 [2048, 1024], P('fs', 'tp'), may hold values from -0.125 to 0.125
- state_value: bfloat16 [2048, 1024], P('fs', 'tp'), may hold values from -0.125 to 0.125
- map_lambda: float32 [8], P('tp'), may hold values from 0.3 to 0.8
- diff_gain: float32 [1024], P('tp'), may hold values from 0.1 to 1.9
- decay_rate: float32 [8], P('tp'), may hold values from 0 to 0.04
- state_gain: float32 [1024], P('tp'), may hold values from 0.1 to 1.9
- out_weight: bfloat16 [2048, 2048], replicated, may hold values from -0.125 to 0.125
Outputs:
- mixed: bfloat16 [4, 1024, 2048], P('fs', ('sp', 'tp'))
All inputs are finite; a program needn't handle non-finite values.
Results may differ from a plain program's by a relative error of at most 0.015.
Values may be sent and summed in bfloat16 or wider, within the bound.
No kernel may reach another device: no remote copies, remote signals or barrier semaphores. Data moves between devices by JAX's collectives and lax.ppermute only.
A program may use at most 128 MiB of HBM per device.

v0:
```python
import jax
import jax.numpy as jnp
from jax import lax
from jax.experimental import pallas as pl
from jax.experimental.pallas import tpu as pltpu
from jax.sharding import PartitionSpec as P


DK = 64
DV = 128
DR = 128


epsilon = 1e-05
branch_scale = 0.8
masked_score = -1e30


def from_behind(x, axis, by):
    size = lax.axis_size(axis)
    pairs = [(i, i + by) for i in range(size) if 0 <= i + by < size]
    return lax.ppermute(x, axis, pairs)


def entering(x, axis, join, neutral):
    place = lax.axis_index(axis)
    gathered = jax.tree.map(
        lambda a, kind: lax.all_gather(a.astype(kind), axis), x, (jnp.bfloat16, jnp.bfloat16)
    )
    state = jax.tree.map(lambda a, e: jnp.zeros_like(a) + jnp.asarray(e, a.dtype), x, neutral)

    def one(turn, state):
        return join(
            state,
            jax.tree.map(
                lambda a, own: lax.dynamic_index_in_dim(a, turn, 0, False).astype(own.dtype),
                gathered,
                x,
            ),
        )

    return lax.fori_loop(0, place, one, state)


def attend(att_query, att_keys, att_values, map_lambda, diff_gain):
    tok_rows = att_query.shape[0]
    head_count = map_lambda.shape[0]
    key_width = att_keys.shape[1]
    query_heads = att_query.reshape(tok_rows, head_count, 2, DK)
    sp_index = lax.axis_index("sp")
    query_place = sp_index * tok_rows + jnp.arange(tok_rows)
    score_scale = DK ** (-0.5)

    def absorb_block(running, inputs):
        key_block, key_place = inputs
        key_heads = key_block[:, :key_width].reshape(tok_rows, head_count, 2, DK)
        value_heads = key_block[:, key_width:].reshape(tok_rows, head_count, DV)
        scores = (
            jnp.einsum(
                "qhmd,khmd->mhqk", query_heads, key_heads, preferred_element_type=jnp.float32
            )
            * score_scale
        )
        causal = key_place[None, :] <= query_place[:, None]
        row_peak, totals, summed = running
        new_peak = jnp.maximum(row_peak, jnp.max(jnp.where(causal, scores, masked_score), axis=-1))
        weights = jnp.where(causal, jnp.exp(scores - new_peak[..., None]), 0.0)
        factor = jnp.exp(row_peak - new_peak)
        totals = totals * factor + jnp.sum(weights, axis=-1)
        summed = summed * factor[..., None] + jnp.einsum(
            "mhqk,khv->mhqv",
            weights.astype(jnp.bfloat16),
            value_heads,
            preferred_element_type=jnp.float32,
        )
        return ((new_peak, totals, summed), None)

    def absorb(running, pieces, first_row):
        piece_rows = pieces.shape[0]
        stacked = pieces.reshape(piece_rows // tok_rows, tok_rows, pieces.shape[1])
        places = (first_row + jnp.arange(piece_rows)).reshape(piece_rows // tok_rows, tok_rows)
        return lax.scan(absorb_block, running, (stacked, places))[0]

    starting = (
        jnp.full((2, head_count, tok_rows), masked_score, jnp.float32),
        jnp.zeros((2, head_count, tok_rows), jnp.float32),
        jnp.zeros((2, head_count, tok_rows, DV), jnp.float32),
    )
    joined_kv = jnp.concatenate([att_keys, att_values], axis=1)
    first_state = absorb(starting, joined_kv, sp_index * tok_rows)

    def relay_step(step_index, relay_state):
        running, moving = relay_state
        moving = from_behind(moving, "sp", 1)
        first_row = (sp_index - step_index) * tok_rows
        running = lax.cond(
            first_row >= 0,
            lambda holding: absorb(holding, moving, first_row),
            lambda holding: holding,
            running,
        )
        return (running, moving)

    running, _ = lax.fori_loop(1, lax.axis_size("sp"), relay_step, (first_state, joined_kv))
    _, totals, summed = running
    averaged = summed / totals[..., None]
    differ = averaged[0] - map_lambda[:, None, None] * averaged[1]
    normed = differ * lax.rsqrt(jnp.mean(differ * differ, axis=-1, keepdims=True) + epsilon)
    normed = normed * diff_gain.reshape(head_count, 1, DV) * branch_scale
    return normed.transpose(1, 0, 2).reshape(tok_rows, head_count * DV).astype(jnp.bfloat16)


def retain(ret_query, ret_keys, ret_values, decay_rate, state_gain):
    tok_rows = ret_query.shape[0]
    head_count = decay_rate.shape[0]
    query_heads = ret_query.reshape(tok_rows, head_count, DR)
    key_heads = ret_keys.reshape(tok_rows, head_count, DR)
    value_heads = ret_values.reshape(tok_rows, head_count, DR)
    position = jnp.arange(tok_rows).astype(jnp.float32)
    distance = position[:, None] - position[None, :]
    decay_col = decay_rate[:, None, None]
    within = jnp.where(distance >= 0, jnp.exp(-decay_col * jnp.maximum(distance, 0.0)), 0.0)
    local_scores = (
        jnp.einsum("qhd,khd->hqk", query_heads, key_heads, preferred_element_type=jnp.float32)
        * within
    )
    intra_out = jnp.einsum(
        "hqk,khv->hqv",
        local_scores.astype(jnp.bfloat16),
        value_heads,
        preferred_element_type=jnp.float32,
    )
    key_decayed = key_heads.astype(jnp.float32) * jnp.exp(
        -decay_rate[None, :, None] * (tok_rows - 1.0 - position)[:, None, None]
    )
    own_state = jnp.einsum(
        "khd,khv->hdv",
        key_decayed,
        value_heads.astype(jnp.float32),
        precision=lax.Precision.HIGHEST,
    )
    block_decay = jnp.exp(-decay_rate * tok_rows)

    def link_states(earlier, later):
        return (earlier[0] * later[1][:, None, None] + later[0], earlier[1] * later[1])

    identity = (jnp.zeros_like(own_state), jnp.ones_like(block_decay))
    incoming, _ = entering((own_state, block_decay), "sp", link_states, identity)
    carried = jnp.einsum(
        "qhd,hdv->hqv", query_heads.astype(jnp.float32), incoming, precision=lax.Precision.HIGHEST
    )
    carried = carried * jnp.exp(-decay_col * (position + 1.0)[None, :, None])
    combined = intra_out + carried
    normed = combined * lax.rsqrt(jnp.mean(combined * combined, axis=-1, keepdims=True) + epsilon)
    normed = normed * state_gain.reshape(head_count, 1, DR)
    return normed.transpose(1, 0, 2).reshape(tok_rows, head_count * DR).astype(jnp.bfloat16)


def body_by_position(
    tokens,
    norm_gain,
    query_weight,
    key_weight,
    value_weight,
    state_query,
    state_key,
    state_value,
    map_lambda,
    diff_gain,
    decay_rate,
    state_gain,
    out_weight,
):
    gathered = lax.all_gather(tokens[0], "tp", axis=1, tiled=True)
    tok_float = gathered.astype(jnp.float32)
    normed = tok_float * lax.rsqrt(
        jnp.mean(tok_float * tok_float, axis=-1, keepdims=True) + epsilon
    )
    normed = (normed * norm_gain).astype(jnp.bfloat16)
    pieces = (
        lax.all_gather(query_weight, "fs", axis=0, tiled=True),
        lax.all_gather(key_weight, "fs", axis=0, tiled=True),
        lax.all_gather(value_weight, "fs", axis=0, tiled=True),
        lax.all_gather(state_query, "fs", axis=0, tiled=True),
        lax.all_gather(state_key, "fs", axis=0, tiled=True),
        lax.all_gather(state_value, "fs", axis=0, tiled=True),
    )
    projected = tuple(
        (jnp.dot(normed, row_block, preferred_element_type=jnp.float32) for row_block in pieces)
    )
    att_query, att_keys, att_values, ret_query, ret_keys, ret_values = (
        member.astype(jnp.bfloat16) for member in projected
    )
    attended = attend(att_query, att_keys, att_values, map_lambda, diff_gain)
    retained = retain(ret_query, ret_keys, ret_values, decay_rate, state_gain)
    joined = jnp.concatenate([attended, retained], axis=1)
    diff_width = attended.shape[1]
    ret_width = retained.shape[1]
    tp_count = lax.axis_size("tp")
    tp_index = lax.axis_index("tp")
    own_rows = jnp.concatenate(
        [
            lax.dynamic_slice_in_dim(out_weight, tp_index * diff_width, diff_width, 0),
            lax.dynamic_slice_in_dim(
                out_weight, tp_count * diff_width + tp_index * ret_width, ret_width, 0
            ),
        ],
        axis=0,
    )
    output = lax.psum_scatter(
        jnp.dot(joined, own_rows, preferred_element_type=jnp.float32).astype(jnp.bfloat16),
        "tp",
        scatter_dimension=0,
        tiled=True,
    )
    return output[None]


def permuted(x, axis, to):
    return lax.ppermute(x, axis, [(i, to(i)) for i in range(lax.axis_size(axis))])


def chain_blocks(x):
    size, pair = lax.axis_size("sp"), lax.axis_size("tp")

    def swap(a, valid):
        pairs = [(s * pair + t, s * pair + 1 - t) for s in valid for t in range(pair)]
        return lax.ppermute(a, ("sp", "tp"), pairs)

    up = down = x
    stages = [[(x, swap(x, range(size)), 0)]]
    for k in range(1, size):
        up = lax.ppermute(up, "sp", [(i, i + 1) for i in range(k - 1, size - 1)])
        down = lax.ppermute(down, "sp", [(i, i - 1) for i in range(1, size - k + 1)])
        from_up = (up, swap(up, range(k, size)), -k)
        stages.append([from_up, (down, swap(down, range(size - k)), k)])
    return stages


def cube_pieces(w, axis):
    send = lambda k: permuted(w, axis, lambda i: i ^ k)
    return [(w, 0)] + [(send(k), k) for k in range(1, lax.axis_size(axis))]


def call(kernel, outs, scratch, scalars, arrays):
    smem = pl.BlockSpec(memory_space=pltpu.SMEM)
    vmem = pl.BlockSpec(memory_space=pltpu.VMEM)
    return pl.pallas_call(
        kernel,
        out_shape=outs,
        in_specs=[smem] * len(scalars) + [vmem] * len(arrays),
        out_specs=jax.tree.map(lambda _: vmem, outs),
        scratch_shapes=scratch,
    )(*scalars, *arrays)


def normalize_stage(stage, gain):
    rows, width = stage[0][0].shape
    size = lax.axis_size("sp")
    arrays = [a for own, other, _ in stage for a in (own, other)]

    def kernel(gain_ref, *refs):
        ins, outs = refs[: len(arrays)], refs[len(arrays) :]
        sp_index, tp_index = lax.axis_index("sp"), lax.axis_index("tp")
        for n, (_, _, offset) in enumerate(stage):
            block = sp_index + offset

            @pl.when((block >= 0) & (block < size))
            def _():
                a = ins[2 * n][...].astype(jnp.float32)
                b = ins[2 * n + 1][...].astype(jnp.float32)
                total = jnp.sum(a * a + b * b, axis=-1, keepdims=True)
                scale = lax.rsqrt(total / (2 * width) + epsilon)
                gain_a = gain_ref[pl.ds(tp_index, 1), :]
                gain_b = gain_ref[pl.ds(1 - tp_index, 1), :]
                outs[n][0] = (a * scale * gain_a).astype(jnp.bfloat16)
                outs[n][1] = (b * scale * gain_b).astype(jnp.bfloat16)

    out = [jax.ShapeDtypeStruct((2, rows, width), jnp.bfloat16)] * len(stage)
    normed = call(kernel, out, [], [], [gain.reshape(2, width)] + arrays)
    return [(a, offset) for a, (_, _, offset) in zip(normed, stage)]


def project(normed_refs, offsets, piece_refs, pieces, weight_ref, qkv_ref):
    _, rows, width = normed_refs[0].shape
    member_rows = pieces[0][0].shape[0]
    sp_index, fs_index, tp_index = (lax.axis_index(a) for a in ("sp", "fs", "tp"))
    for ref, (_, k) in zip(piece_refs, pieces):
        weight_ref[pl.ds((fs_index ^ k) * member_rows, member_rows), :] = ref[...]
    for ref, offset in zip(normed_refs, offsets):
        block = sp_index + offset

        @pl.when((block >= 0) & (block * rows < qkv_ref.shape[0]))
        def _():
            own = weight_ref[pl.ds(tp_index * width, width), :]
            other = weight_ref[pl.ds((1 - tp_index) * width, width), :]
            result = jnp.dot(ref[0], own, preferred_element_type=jnp.float32)
            result += jnp.dot(ref[1], other, preferred_element_type=jnp.float32)
            qkv_ref[pl.ds(block * rows, rows), :] = result.astype(jnp.bfloat16)


def mix_head(kernel_of, scalars, gain, normed, pieces):
    _, rows, width = normed[0][0].shape
    size = lax.axis_size("sp")
    columns = pieces[0][0].shape[1]
    head_width = gain.shape[0] // size
    offsets = [offset for _, offset in normed]

    def kernel(scalar_ref, gain_ref, *refs):
        normed_refs, refs = refs[: len(normed)], refs[len(normed) :]
        piece_refs, refs = refs[: len(pieces)], refs[len(pieces) :]
        out_refs, (weight_ref, qkv_ref, mixed_ref) = refs[:size], refs[size:]
        project(normed_refs, offsets, piece_refs, pieces, weight_ref, qkv_ref)
        sp_index = lax.axis_index("sp")

        def store(block, value):
            ahead = lax.rem(block - sp_index + size, size)
            mixed_ref[pl.ds(ahead * rows, rows), :] = value

        kernel_of(scalar_ref[sp_index], gain_ref[pl.ds(sp_index, 1), :], qkv_ref, rows, store)
        for k, ref in enumerate(out_refs):
            ref[...] = mixed_ref[k * rows : (k + 1) * rows, :]

    length = size * rows
    return call(
        kernel,
        [jax.ShapeDtypeStruct((rows, head_width), jnp.bfloat16)] * size,
        [
            pltpu.VMEM((2 * width, columns), jnp.bfloat16),
            pltpu.VMEM((length, columns), jnp.bfloat16),
            pltpu.VMEM((length, head_width), jnp.bfloat16),
        ],
        [scalars],
        [gain.reshape(size, head_width)] + [a for a, _ in normed] + [p[0] for p in pieces],
    )


def exchange_positions(blocks):
    size = lax.axis_size("sp")
    got = [blocks[0]] + [
        permuted(blocks[k], "sp", lambda i: (i + k) % size) for k in range(1, size)
    ]
    return got


def exchange_halves(got):
    rows, width = got[0].shape
    half = rows // 2

    def kernel(*refs):
        ins, (mine_ref, theirs_ref) = refs[:-2], refs[-2:]
        tp_index = lax.axis_index("tp")
        for k, ref in enumerate(ins):
            at = slice(k * width, (k + 1) * width)
            mine_ref[:, at] = ref[pl.ds(tp_index * half, half), :]
            theirs_ref[:, at] = ref[pl.ds((1 - tp_index) * half, half), :]

    out = [jax.ShapeDtypeStruct((half, width * len(got)), got[0].dtype)] * 2
    mine, theirs = call(kernel, out, [], [], got)
    return mine, permuted(theirs, "tp", lambda i: 1 - i)


def output_product(pairs, out_weight):
    size = lax.axis_size("sp")
    rows = pairs[0][0].shape[0]
    head_width = pairs[0][0].shape[1] // size

    def kernel(weight_ref, *refs):
        ins, (out_ref, left_ref) = refs[:-2], refs[-2:]
        sp_index, tp_index = lax.axis_index("sp"), lax.axis_index("tp")
        columns = size * head_width
        for n, ref in enumerate(ins):
            side = tp_index if n % 2 == 0 else 1 - tp_index
            for k in range(size):
                head = lax.rem(sp_index - k + size, size)
                at = (n // 2 * 2 + side) * columns + head * head_width
                left_ref[:, pl.ds(pl.multiple_of(at, head_width), head_width)] = ref[
                    :, k * head_width : (k + 1) * head_width
                ]
        out_ref[...] = jnp.dot(
            left_ref[...], weight_ref[...], preferred_element_type=jnp.float32
        ).astype(jnp.bfloat16)

    return call(
        kernel,
        jax.ShapeDtypeStruct((rows, out_weight.shape[1]), jnp.bfloat16),
        [pltpu.VMEM((rows, out_weight.shape[0]), jnp.bfloat16)],
        [],
        [out_weight] + [a for pair in pairs for a in pair],
    )


def dot_t(a, b):
    return lax.dot_general(a, b, (((1,), (1,)), ((), ())), preferred_element_type=jnp.float32)


def attend_head(mix, gain, qkv_ref, rows, store):
    score_scale = DK ** (-0.5)
    lane = lax.broadcasted_iota(jnp.int32, (rows, 2 * DK), 1)
    below = lax.broadcasted_iota(jnp.int32, (rows, rows), 0) >= lax.broadcasted_iota(
        jnp.int32, (rows, rows), 1
    )
    for block in range(qkv_ref.shape[0] // rows):
        at = slice(block * rows, (block + 1) * rows)
        query = qkv_ref[at, : 2 * DK]
        outs = []
        for m in range(2):
            mine = (lane >= DK) if m else (lane < DK)
            part = jnp.where(mine, query, jnp.zeros_like(query))
            scores = dot_t(part, qkv_ref[at, 2 * DK : 4 * DK])
            scores = jnp.where(below, scores * score_scale, masked_score)
            peak = jnp.max(scores, axis=-1, keepdims=True)
            if block:
                past = slice(0, block * rows)
                before = dot_t(part, qkv_ref[past, 2 * DK : 4 * DK]) * score_scale
                peak = jnp.maximum(peak, jnp.max(before, axis=-1, keepdims=True))
            weights = jnp.exp(scores - peak)
            total = jnp.sum(weights, axis=-1, keepdims=True)
            summed = jnp.dot(
                weights.astype(jnp.bfloat16),
                qkv_ref[at, 4 * DK :],
                preferred_element_type=jnp.float32,
            )
            if block:
                weights = jnp.exp(before - peak)
                total += jnp.sum(weights, axis=-1, keepdims=True)
                summed += jnp.dot(
                    weights.astype(jnp.bfloat16),
                    qkv_ref[past, 4 * DK :],
                    preferred_element_type=jnp.float32,
                )
            outs.append(summed / total)
        differ = outs[0] - mix * outs[1]
        scale = lax.rsqrt(jnp.mean(differ * differ, axis=-1, keepdims=True) + epsilon)
        store(block, (differ * scale * gain * branch_scale).astype(jnp.bfloat16))


def split_high_low(x):
    high = x.astype(jnp.bfloat16)
    return high, (x - high.astype(jnp.float32)).astype(jnp.bfloat16)


def retain_head(r, gain, qkv_ref, rows, store):
    length = qkv_ref.shape[0]
    distance = lax.broadcasted_iota(jnp.int32, (rows, rows), 0) - lax.broadcasted_iota(
        jnp.int32, (rows, rows), 1
    )
    far = jnp.maximum(distance, 0).astype(jnp.float32)
    within = jnp.where(distance >= 0, jnp.exp(-r * far), 0.0)
    position = lax.broadcasted_iota(jnp.int32, (rows, DR), 0).astype(jnp.float32)
    query_decay = jnp.exp(-r * (position + 1.0))
    key_decay = jnp.exp(-r * (rows - 1.0 - position))
    block_decay = jnp.exp(jnp.full((DR, DR), -r * rows, jnp.float32))
    state = None
    for block in range(length // rows):
        at = slice(block * rows, (block + 1) * rows)
        query = qkv_ref[at, :DR]
        key = qkv_ref[at, DR : 2 * DR]
        value = qkv_ref[at, 2 * DR :]
        local = (dot_t(query, key) * within).astype(jnp.bfloat16)
        total = jnp.dot(local, value, preferred_element_type=jnp.float32)
        if block:
            high, low = split_high_low(state)
            carried = jnp.dot(query, high, preferred_element_type=jnp.float32)
            carried += jnp.dot(query, low, preferred_element_type=jnp.float32)
            total += carried * query_decay
        if (block + 1) * rows < length:
            high, low = split_high_low(key.astype(jnp.float32) * key_decay)
            contract = (((0,), (0,)), ((), ()))
            fresh = lax.dot_general(high, value, contract, preferred_element_type=jnp.float32)
            fresh += lax.dot_general(low, value, contract, preferred_element_type=jnp.float32)
            state = fresh if state is None else state * block_decay + fresh
        scale = lax.rsqrt(jnp.mean(total * total, axis=-1, keepdims=True) + epsilon)
        store(block, (total * scale * gain).astype(jnp.bfloat16))


def body_by_head(
    tokens,
    norm_gain,
    query_weight,
    key_weight,
    value_weight,
    state_query,
    state_key,
    state_value,
    map_lambda,
    diff_gain,
    decay_rate,
    state_gain,
    out_weight,
):
    sp_index = lax.axis_index("sp")

    def head_columns(*weights):
        each = weights[0].shape[1] // map_lambda.shape[0]
        return jnp.concatenate(
            [lax.dynamic_slice_in_dim(w, sp_index * each, each, 1) for w in weights], axis=1
        )

    att_own = head_columns(query_weight, key_weight, value_weight)
    ret_own = head_columns(state_query, state_key, state_value)
    stages = chain_blocks(tokens[0])
    att_pieces = cube_pieces(att_own, "fs")
    ret_pieces = cube_pieces(ret_own, "fs")
    normed = []
    for stage in stages:
        normed += normalize_stage(stage, norm_gain)
    attended = mix_head(attend_head, map_lambda, diff_gain, normed, att_pieces)
    attended = exchange_positions(attended)
    retained = mix_head(retain_head, decay_rate, state_gain, normed, ret_pieces)
    retained = exchange_positions(retained)
    pairs = [exchange_halves(attended), exchange_halves(retained)]
    return output_product(pairs, out_weight)[None]


def by_head(mesh, map_lambda, decay_rate):
    size = mesh.shape
    power = size["fs"] & (size["fs"] - 1) == 0
    heads = size["sp"] * size["tp"]
    same = map_lambda.shape[0] == heads and decay_rate.shape[0] == heads
    return power and size["tp"] == 2 and same


def solution(mesh):
    placed = (
        P("fs", "sp", "tp"),
        P(),
        P("fs", "tp"),
        P("fs", "tp"),
        P("fs", "tp"),
        P("fs", "tp"),
        P("fs", "tp"),
        P("fs", "tp"),
        P("tp"),
        P("tp"),
        P("tp"),
        P("tp"),
        P(),
    )

    def run(*arrays):
        split = by_head(mesh, arrays[8], arrays[10])

        def body(*own):
            if not split:
                return body_by_position(*own)
            return body_by_head(*own)

        return jax.shard_map(
            body, mesh=mesh, in_specs=placed, out_specs=P("fs", ("sp", "tp"), None), check_vma=False
        )(*arrays)

    return run
```

profile of v0, /device:TPU:0, one launch (start us, length us, event | category | flops | bytes accessed | tf_op | source)
XLA Modules:
  0.0 119.4 jit_solution(11840453919104812748)
XLA Ops:
  0.0 5.1 %collective-permute-start.1 = (bf16[256,1024]{1,0:T(8,128)(2,1)}, bf16[256,1024]{1,0:T(8,128)(2,1)S(1)}, u32[]{:S(2)}, u32[]{:S(2)}) collective-permute-start(bf16[256,1024]{1,0:T(8,128)(2,1)} %bitcast.4), channel_id=1, source_target_pairs={{0,8},{8,16},{16,24},{1,9},{9,17},{17,25},{2,10},{10,18},{18,26},{... | collective-permute-start | bytes 1572872 | tf_op jit(solution)/shard_map/ppermute | solution.py:233
  5.1 1.3 %collective-permute-start.3 = (bf16[256,1024]{1,0:T(8,128)(2,1)}, bf16[256,1024]{1,0:T(8,128)(2,1)S(1)}, u32[]{:S(2)}, u32[]{:S(2)}) collective-permute-start(bf16[256,1024]{1,0:T(8,128)(2,1)} %bitcast.5), channel_id=1, source_target_pairs={{8,0},{16,8},{24,16},{9,1},{17,9},{25,17},{10,2},{18,10},{26,18},{... | collective-permute-start | bytes 1572872 | tf_op jit(solution)/shard_map/ppermute | solution.py:234
  6.4 10.1 %collective-permute-done.1.refs_0_ = bf16[256,1024]{1,0:T(8,128)(2,1)S(1)} collective-permute-done((bf16[256,1024]{1,0:T(8,128)(2,1)}, bf16[256,1024]{1,0:T(8,128)(2,1)S(1)}, u32[]{:S(2)}, u32[]{:S(2)}) %collective-permute-start.1) | collective-permute-done | bytes 524320 | tf_op jit(solution)/shard_map/ppermute | solution.py:233
  16.6 0.7 collective-permute-start.5
  17.3 3.4 %collective-permute-done.3.refs_2_ = bf16[256,1024]{1,0:T(8,128)(2,1)S(1)} collective-permute-done((bf16[256,1024]{1,0:T(8,128)(2,1)}, bf16[256,1024]{1,0:T(8,128)(2,1)S(1)}, u32[]{:S(2)}, u32[]{:S(2)}) %collective-permute-start.3) | collective-permute-done | bytes 524320 | tf_op jit(solution)/shard_map/ppermute | solution.py:234
  20.6 1.3 %collective-permute-start.7 = (bf16[256,1024]{1,0:T(8,128)(2,1)S(1)}, bf16[256,1024]{1,0:T(8,128)(2,1)S(1)}, u32[]{:S(2)}, u32[]{:S(2)}) collective-permute-start(bf16[256,1024]{1,0:T(8,128)(2,1)S(1)} %collective-permute-done.3.refs_2_), channel_id=1, source_target_pairs={{8,0},{16,8},{9,1},{17,9},{10,2},{18,10},{11,3},{19,11},{12,4},{20... | collective-permute-start | bytes 1572872 | tf_op jit(solution)/shard_map/ppermute | solution.py:234
  22.0 1.0 constant_dynamic-slice_fusion.3
  23.0 0.7 collective-permute-start.2
  23.8 0.7 collective-permute-start.9
  24.5 10.7 %collective-permute-done.7.refs_2_ = bf16[256,1024]{1,0:T(8,128)(2,1)S(1)} collective-permute-done((bf16[256,1024]{1,0:T(8,128)(2,1)S(1)}, bf16[256,1024]{1,0:T(8,128)(2,1)S(1)}, u32[]{:S(2)}, u32[]{:S(2)}) %collective-permute-start.7) | collective-permute-done | bytes 524320 | tf_op jit(solution)/shard_map/ppermute | solution.py:234
  35.2 1.3 %collective-permute-start.11 = (bf16[256,1024]{1,0:T(8,128)(2,1)S(1)}, bf16[256,1024]{1,0:T(8,128)(2,1)S(1)}, u32[]{:S(2)}, u32[]{:S(2)}) collective-permute-start(bf16[256,1024]{1,0:T(8,128)(2,1)S(1)} %collective-permute-done.7.refs_2_), channel_id=1, source_target_pairs={{8,0},{9,1},{10,2},{11,3},{12,4},{13,5},{14,6},{15,7}} | collective-permute-start | bytes 1572872 | tf_op jit(solution)/shard_map/ppermute | solution.py:234
  36.5 1.6 %collective-permute-start.13 = (bf16[512,384]{1,0:T(8,128)(2,1)S(1)}, bf16[512,384]{1,0:T(8,128)(2,1)S(1)}, u32[]{:S(2)}, u32[]{:S(2)}) collective-permute-start(bf16[512,384]{1,0:T(8,128)(2,1)S(1)} %pad_maximum_fusion.refs_7_), channel_id=1, source_target_pairs={{0,2},{2,0},{4,6},{6,4},{1,3},{3,1},{5,7},{7,5},{8,10},{10,8},{12,... | collective-permute-start | bytes 1179656 | tf_op jit(solution)/shard_map/ppermute | solution.py:220
  38.1 7.5 %collective-permute-done.13.refs_8_ = bf16[512,384]{1,0:T(8,128)(2,1)S(1)} collective-permute-done((bf16[512,384]{1,0:T(8,128)(2,1)S(1)}, bf16[512,384]{1,0:T(8,128)(2,1)S(1)}, u32[]{:S(2)}, u32[]{:S(2)}) %collective-permute-start.13) | collective-permute-done | bytes 393248 | tf_op jit(solution)/shard_map/ppermute | solution.py:220
  45.6 1.9 %collective-permute-start.4 = (bf16[256,1024]{1,0:T(8,128)(2,1)S(1)}, bf16[256,1024]{1,0:T(8,128)(2,1)S(1)}, u32[]{:S(2)}, u32[]{:S(2)}) collective-permute-start(bf16[256,1024]{1,0:T(8,128)(2,1)S(1)} %collective-permute-done.3.refs_2_), channel_id=1, source_target_pairs={{0,1},{1,0},{8,9},{9,8},{16,17},{17,16},{2,3},{3,2},{10,11},{11,10... | collective-permute-start | bytes 1572872 | tf_op jit(solution)/shard_map/ppermute | solution.py:228
  47.5 0.7 collective-permute-start.6
  48.2 2.4 %collective-permute-start.8 = (bf16[256,1024]{1,0:T(8,128)(2,1)S(1)}, bf16[256,1024]{1,0:T(8,128)(2,1)S(1)}, u32[]{:S(2)}, u32[]{:S(2)}) collective-permute-start(bf16[256,1024]{1,0:T(8,128)(2,1)S(1)} %collective-permute-done.7.refs_2_), channel_id=1, source_target_pairs={{0,1},{1,0},{8,9},{9,8},{2,3},{3,2},{10,11},{11,10},{4,5},{5,4},{1... | collective-permute-start | bytes 1572872 | tf_op jit(solution)/shard_map/ppermute | solution.py:228
  50.7 0.7 collective-permute-start.10
  51.4 1.9 %collective-permute-start.12 = (bf16[256,1024]{1,0:T(8,128)(2,1)S(1)}, bf16[256,1024]{1,0:T(8,128)(2,1)S(1)}, u32[]{:S(2)}, u32[]{:S(2)}) collective-permute-start(bf16[256,1024]{1,0:T(8,128)(2,1)S(1)} %collective-permute-done.11.refs_2_), channel_id=1, source_target_pairs={{0,1},{1,0},{2,3},{3,2},{4,5},{5,4},{6,7},{7,6}} | collective-permute-start | bytes 1572872 | tf_op jit(solution)/shard_map/ppermute | solution.py:228
  53.3 0.9 constant_dynamic-slice_fusion.2
  54.3 1.0 constant_dynamic-slice_fusion
  55.3 1.6 %collective-permute-start.14 = (bf16[512,384]{1,0:T(8,128)(2,1)S(1)}, bf16[512,384]{1,0:T(8,128)(2,1)}, u32[]{:S(2)}, u32[]{:S(2)}) collective-permute-start(bf16[512,384]{1,0:T(8,128)(2,1)S(1)} %pad_maximum_fusion.refs_7_), channel_id=1, source_target_pairs={{0,4},{2,6},{4,0},{6,2},{1,5},{3,7},{5,1},{7,3},{8,12},{10,14},{12... | collective-permute-start | bytes 1179656 | tf_op jit(solution)/shard_map/ppermute | solution.py:220
  56.9 1.4 %collective-permute-start.15 = (bf16[512,384]{1,0:T(8,128)(2,1)S(1)}, bf16[512,384]{1,0:T(8,128)(2,1)}, u32[]{:S(2)}, u32[]{:S(2)}) collective-permute-start(bf16[512,384]{1,0:T(8,128)(2,1)S(1)} %pad_maximum_fusion.refs_7_), channel_id=1, source_target_pairs={{0,6},{2,4},{4,2},{6,0},{1,7},{3,5},{5,3},{7,1},{8,14},{10,12},{12... | collective-permute-start | bytes 1179656 | tf_op jit(solution)/shard_map/ppermute | solution.py:220
  58.4 0.9 collective-permute-start.20
  59.3 1.2 %collective-permute-start.21 = (bf16[512,384]{1,0:T(8,128)(2,1)S(1)}, bf16[512,384]{1,0:T(8,128)(2,1)}, u32[]{:S(2)}, u32[]{:S(2)}) collective-permute-start(bf16[512,384]{1,0:T(8,128)(2,1)S(1)} %pad_maximum_fusion.1.refs_7_), channel_id=1, source_target_pairs={{0,4},{2,6},{4,0},{6,2},{1,5},{3,7},{5,1},{7,3},{8,12},{10,14},{12... | collective-permute-start | bytes 1179656 | tf_op jit(solution)/shard_map/ppermute | solution.py:220
  60.6 0.8 copy-done.14
  61.4 1.7 %collective-permute-start.22 = (bf16[512,384]{1,0:T(8,128)(2,1)S(1)}, bf16[512,384]{1,0:T(8,128)(2,1)}, u32[]{:S(2)}, u32[]{:S(2)}) collective-permute-start(bf16[512,384]{1,0:T(8,128)(2,1)S(1)} %pad_maximum_fusion.1.refs_7_), channel_id=1, source_target_pairs={{0,6},{2,4},{4,2},{6,0},{1,7},{3,5},{5,3},{7,1},{8,14},{10,12},{12... | collective-permute-start | bytes 1179656 | tf_op jit(solution)/shard_map/ppermute | solution.py:220
  63.1 1.3 %reshape.13.gain_ref = f32[2,1024]{1,0:T(2,128)} reshape(f32[2048]{0:T(1024)} %param.14) | data formatting | bytes 16384 | tf_op jit(solution)/shard_map/reshape | solution.py:280
  64.4 2.6 %shard_map.127.refs_0_ = bf16[2,256,1024]{2,1,0:T(8,128)(2,1)} custom-call(f32[2,1024]{1,0:T(2,128)} %reshape.13.gain_ref, bf16[256,1024]{1,0:T(8,128)(2,1)} %bitcast.7, bf16[256,1024]{1,0:T(8,128)(2,1)} %collective-permute-done.refs_1_), custom_call_target="tpu_custom_call" | custom-call | tf_op jit(solution)/shard_map/pallas_call | solution.py:248
  67.0 3.3 %shard_map.128 = (bf16[2,256,1024]{2,1,0:T(8,128)(2,1)}, bf16[2,256,1024]{2,1,0:T(8,128)(2,1)}) custom-call(f32[2,1024]{1,0:T(2,128)} %reshape.13.gain_ref, bf16[256,1024]{1,0:T(8,128)(2,1)} %copy-done.3, bf16[256,1024]{1,0:T(8,128)(2,1)} %copy-done.8, bf16[256,1024]{1,0:T(8,128)(2,1)} %copy-done.4, bf16[256,1024]{1,0:T(8,128)(2,1)} %copy-done.10), custom_call_target="tpu_custom_call" | custom-call | tf_op jit(solution)/shard_map/pallas_call | solution.py:248
  70.3 3.3 %shard_map.129 = (bf16[2,256,1024]{2,1,0:T(8,128)(2,1)}, bf16[2,256,1024]{2,1,0:T(8,128)(2,1)}) custom-call(f32[2,1024]{1,0:T(2,128)} %reshape.13.gain_ref, bf16[256,1024]{1,0:T(8,128)(2,1)} %copy-done.5, bf16[256,1024]{1,0:T(8,128)(2,1)} %copy-done.11, bf16[256,1024]{1,0:T(8,128)(2,1)} %copy-done.6, bf16[256,1024]{1,0:T(8,128)(2,1)} %copy-done.12), custom_call_target="tpu_custom_call" | custom-call | tf_op jit(solution)/shard_map/pallas_call | solution.py:248
  73.6 3.2 %shard_map.130 = (bf16[2,256,1024]{2,1,0:T(8,128)(2,1)}, bf16[2,256,1024]{2,1,0:T(8,128)(2,1)}) custom-call(f32[2,1024]{1,0:T(2,128)} %reshape.13.gain_ref, bf16[256,1024]{1,0:T(8,128)(2,1)} %copy-done.7, bf16[256,1024]{1,0:T(8,128)(2,1)} %copy-done.13, bf16[256,1024]{1,0:T(8,128)(2,1)} %copy-done.9, bf16[256,1024]{1,0:T(8,128)(2,1)} %copy-done.14), custom_call_target="tpu_custom_call" | custom-call | tf_op jit(solution)/shard_map/pallas_call | solution.py:248
  76.9 10.8 %shard_map.131 = (bf16[256,128]{1,0:T(8,128)(2,1)}, bf16[256,128]{1,0:T(8,128)(2,1)}, bf16[256,128]{1,0:T(8,128)(2,1)}, bf16[256,128]{1,0:T(8,128)(2,1)}) custom-call(f32[4]{0:T(128)} %scalar_ref.2, f32[4,128]{1,0:T(4,128)} %bitcast.8, bf16[2,256,1024]{2,1,0:T(8,128)(2,1)} %shard_map.127.refs_0_, bf16[2,256,1024]{2,1,0:T(8,128)(2,1)} %get-tuple-element.23.refs_1_, ...), custom_call_target="tpu_custom_call" | custom-call | tf_op jit(solution)/shard_map/pallas_call | solution.py:248
  87.7 1.2 %collective-permute-start.16 = (bf16[256,128]{1,0:T(8,128)(2,1)}, bf16[256,128]{1,0:T(8,128)(2,1)S(1)}, u32[]{:S(2)}, u32[]{:S(2)}) collective-permute-start(bf16[256,128]{1,0:T(8,128)(2,1)} %get-tuple-element.30), channel_id=1, source_target_pairs={{0,8},{8,16},{16,24},{24,0},{1,9},{9,17},{17,25},{25,1},{2,10},{10... | collective-permute-start | bytes 196616 | tf_op jit(solution)/shard_map/ppermute | solution.py:220
  88.9 2.8 %collective-permute-start.18 = (bf16[256,128]{1,0:T(8,128)(2,1)}, bf16[256,128]{1,0:T(8,128)(2,1)S(1)}, u32[]{:S(2)}, u32[]{:S(2)}) collective-permute-start(bf16[256,128]{1,0:T(8,128)(2,1)} %get-tuple-element.32), channel_id=1, source_target_pairs={{0,24},{8,0},{16,8},{24,16},{1,25},{9,1},{17,9},{25,17},{2,26},{10... | collective-permute-start | bytes 196616 | tf_op jit(solution)/shard_map/ppermute | solution.py:220
  91.8 0.5 collective-permute-done.21.refs_9_
  92.2 8.5 %shard_map.133 = (bf16[256,128]{1,0:T(8,128)(2,1)}, bf16[256,128]{1,0:T(8,128)(2,1)}, bf16[256,128]{1,0:T(8,128)(2,1)}, bf16[256,128]{1,0:T(8,128)(2,1)}) custom-call(f32[4]{0:T(128)} %scalar_ref.3, f32[4,128]{1,0:T(4,128)} %bitcast.9, bf16[2,256,1024]{2,1,0:T(8,128)(2,1)} %shard_map.127.refs_0_, bf16[2,256,1024]{2,1,0:T(8,128)(2,1)} %get-tuple-element.23.refs_1_, ...), custom_call_target="tpu_custom_call" | custom-call | tf_op jit(solution)/shard_map/pallas_call | solution.py:248
  100.8 0.7 collective-permute-start.23
  101.5 1.0 collective-permute-start.24
  102.4 2.7 %collective-permute-start.25 = (bf16[256,128]{1,0:T(8,128)(2,1)}, bf16[256,128]{1,0:T(8,128)(2,1)S(1)}, u32[]{:S(2)}, u32[]{:S(2)}) collective-permute-start(bf16[256,128]{1,0:T(8,128)(2,1)} %get-tuple-element.38), channel_id=1, source_target_pairs={{0,24},{8,0},{16,8},{24,16},{1,25},{9,1},{17,9},{25,17},{2,26},{10... | collective-permute-start | bytes 196616 | tf_op jit(solution)/shard_map/ppermute | solution.py:220
  105.1 0.6 copy-done.19
  105.7 1.7 %shard_map.132 = (bf16[128,512]{1,0:T(8,128)(2,1)}, bf16[128,512]{1,0:T(8,128)(2,1)}) custom-call(bf16[256,128]{1,0:T(8,128)(2,1)} %get-tuple-element.29.refs_0_, bf16[256,128]{1,0:T(8,128)(2,1)} %copy-done.18, bf16[256,128]{1,0:T(8,128)(2,1)} %copy-done.19, bf16[256,128]{1,0:T(8,128)(2,1)} %copy-done.20), custom_call_target="tpu_custom_call" | custom-call | tf_op jit(solution)/shard_map/pallas_call | solution.py:248
  107.4 0.3 collective-permute-done.23.refs_1_
  107.8 1.4 %collective-permute-done.24.refs_2_ = bf16[256,128]{1,0:T(8,128)(2,1)S(1)} collective-permute-done((bf16[256,128]{1,0:T(8,128)(2,1)}, bf16[256,128]{1,0:T(8,128)(2,1)S(1)}, u32[]{:S(2)}, u32[]{:S(2)}) %collective-permute-start.24) | collective-permute-done | bytes 65568 | tf_op jit(solution)/shard_map/ppermute | solution.py:220
  109.2 0.6 copy-done.22
  109.9 1.7 %shard_map.134 = (bf16[128,512]{1,0:T(8,128)(2,1)}, bf16[128,512]{1,0:T(8,128)(2,1)}) custom-call(bf16[256,128]{1,0:T(8,128)(2,1)} %get-tuple-element.35.refs_0_, bf16[256,128]{1,0:T(8,128)(2,1)} %copy-done.21, bf16[256,128]{1,0:T(8,128)(2,1)} %copy-done.22, bf16[256,128]{1,0:T(8,128)(2,1)} %copy-done.23), custom_call_target="tpu_custom_call" | custom-call | tf_op jit(solution)/shard_map/pallas_call | solution.py:248
  111.6 1.5 %collective-permute-done.26.refs_3_ = bf16[128,512]{1,0:T(8,128)(2,1)S(1)} collective-permute-done((bf16[128,512]{1,0:T(8,128)(2,1)}, bf16[128,512]{1,0:T(8,128)(2,1)S(1)}, u32[]{:S(2)}, u32[]{:S(2)}) %collective-permute-start.26) | collective-permute-done | bytes 131104 | tf_op jit(solution)/shard_map/ppermute | solution.py:220
  113.1 0.6 copy-done.17
  113.7 5.7 %shard_map.135 = bf16[128,2048]{1,0:T(8,128)(2,1)} custom-call(bf16[2048,2048]{1,0:T(8,128)(2,1)} %weight_ref.1, bf16[128,512]{1,0:T(8,128)(2,1)} %get-tuple-element.33.refs_0_, bf16[128,512]{1,0:T(8,128)(2,1)} %copy-done.16, bf16[128,512]{1,0:T(8,128)(2,1)} %get-tuple-element.39.refs_2_, bf16[128,512]{1,0:T(8,128)(2,1)} %copy-done.17), custom_call_target="tpu_custom_call" | custom-call | tf_op jit(solution)/shard_map/pallas_call | solution.py:248
  (70 shorter events, 0.4 us)
Async XLA Ops:
  0.0 23.0 %copy-start = (bf16[512,512]{1,0:T(8,128)(2,1)S(1)}, bf16[512,512]{1,0:T(8,128)(2,1)}, u32[]{:S(2)}) copy-start(bf16[512,512]{1,0:T(8,128)(2,1)} %param.15) | copy-start | bytes 1572868
  0.0 16.6 %collective-permute-start.1 = (bf16[256,1024]{1,0:T(8,128)(2,1)}, bf16[256,1024]{1,0:T(8,128)(2,1)S(1)}, u32[]{:S(2)}, u32[]{:S(2)}) collective-permute-start(bf16[256,1024]{1,0:T(8,128)(2,1)} %bitcast.4), channel_id=1, source_target_pairs={{0,8},{8,16},{16,24},{1,9},{9,17},{17,25},{2,10},{10,18},{18,26},{... | collective-permute-start | bytes 1572872 | tf_op jit(solution)/shard_map/ppermute | solution.py:233
  5.1 15.5 %collective-permute-start.3 = (bf16[256,1024]{1,0:T(8,128)(2,1)}, bf16[256,1024]{1,0:T(8,128)(2,1)S(1)}, u32[]{:S(2)}, u32[]{:S(2)}) collective-permute-start(bf16[256,1024]{1,0:T(8,128)(2,1)} %bitcast.5), channel_id=1, source_target_pairs={{8,0},{16,8},{24,16},{9,1},{17,9},{25,17},{10,2},{18,10},{26,18},{... | collective-permute-start | bytes 1572872 | tf_op jit(solution)/shard_map/ppermute | solution.py:234
  16.6 50.4 %copy-start.3 = (bf16[256,1024]{1,0:T(8,128)(2,1)}, bf16[256,1024]{1,0:T(8,128)(2,1)S(1)}, u32[]{:S(2)}) copy-start(bf16[256,1024]{1,0:T(8,128)(2,1)S(1)} %collective-permute-done.1.refs_0_) | copy-start | bytes 1572868
  16.6 7.2 %collective-permute-start.5 = (bf16[256,1024]{1,0:T(8,128)(2,1)S(1)}, bf16[256,1024]{1,0:T(8,128)(2,1)S(1)}, u32[]{:S(2)}, u32[]{:S(2)}) collective-permute-start(bf16[256,1024]{1,0:T(8,128)(2,1)S(1)} %collective-permute-done.1.refs_0_), channel_id=1, source_target_pairs={{8,16},{16,24},{9,17},{17,25},{10,18},{18,26},{11,19},{19,27},{12,... | collective-permute-start | bytes 1572872 | tf_op jit(solution)/shard_map/ppermute | solution.py:233
  20.6 46.4 %copy-start.4 = (bf16[256,1024]{1,0:T(8,128)(2,1)}, bf16[256,1024]{1,0:T(8,128)(2,1)S(1)}, u32[]{:S(2)}) copy-start(bf16[256,1024]{1,0:T(8,128)(2,1)S(1)} %collective-permute-done.3.refs_2_) | copy-start | bytes 1572868
  20.6 14.6 %collective-permute-start.7 = (bf16[256,1024]{1,0:T(8,128)(2,1)S(1)}, bf16[256,1024]{1,0:T(8,128)(2,1)S(1)}, u32[]{:S(2)}, u32[]{:S(2)}) collective-permute-start(bf16[256,1024]{1,0:T(8,128)(2,1)S(1)} %collective-permute-done.3.refs_2_), channel_id=1, source_target_pairs={{8,0},{16,8},{9,1},{17,9},{10,2},{18,10},{11,3},{19,11},{12,4},{20... | collective-permute-start | bytes 1572872 | tf_op jit(solution)/shard_map/ppermute | solution.py:234
  21.9 25.6 %collective-permute-start = (bf16[256,1024]{1,0:T(8,128)(2,1)}, bf16[256,1024]{1,0:T(8,128)(2,1)}, u32[]{:S(2)}, u32[]{:S(2)}) collective-permute-start(bf16[256,1024]{1,0:T(8,128)(2,1)} %bitcast.6), channel_id=1, source_target_pairs={{0,1},{1,0},{8,9},{9,8},{16,17},{17,16},{24,25},{25,24},{2,3},{3,2... | collective-permute-start | bytes 1572872 | tf_op jit(solution)/shard_map/ppermute | solution.py:228
  23.0 25.2 %collective-permute-start.2 = (bf16[256,1024]{1,0:T(8,128)(2,1)S(1)}, bf16[256,1024]{1,0:T(8,128)(2,1)S(1)}, u32[]{:S(2)}, u32[]{:S(2)}) collective-permute-start(bf16[256,1024]{1,0:T(8,128)(2,1)S(1)} %collective-permute-done.1.refs_0_), channel_id=1, source_target_pairs={{8,9},{9,8},{16,17},{17,16},{24,25},{25,24},{10,11},{11,10},{18,19... | collective-permute-start | bytes 1572872 | tf_op jit(solution)/shard_map/ppermute | solution.py:228
  23.7 46.6 %copy-start.5 = (bf16[256,1024]{1,0:T(8,128)(2,1)}, bf16[256,1024]{1,0:T(8,128)(2,1)S(1)}, u32[]{:S(2)}) copy-start(bf16[256,1024]{1,0:T(8,128)(2,1)S(1)} %collective-permute-done.5.refs_0_) | copy-start | bytes 1572868
  23.8 26.9 %collective-permute-start.9 = (bf16[256,1024]{1,0:T(8,128)(2,1)S(1)}, bf16[256,1024]{1,0:T(8,128)(2,1)S(1)}, u32[]{:S(2)}, u32[]{:S(2)}) collective-permute-start(bf16[256,1024]{1,0:T(8,128)(2,1)S(1)} %collective-permute-done.5.refs_0_), channel_id=1, source_target_pairs={{16,24},{17,25},{18,26},{19,27},{20,28},{21,29},{22,30},{23,31}} | collective-permute-start | bytes 1572872 | tf_op jit(solution)/shard_map/ppermute | solution.py:233
  35.2 35.1 %copy-start.6 = (bf16[256,1024]{1,0:T(8,128)(2,1)}, bf16[256,1024]{1,0:T(8,128)(2,1)S(1)}, u32[]{:S(2)}) copy-start(bf16[256,1024]{1,0:T(8,128)(2,1)S(1)} %collective-permute-done.7.refs_2_) | copy-start | bytes 1572868
  35.2 16.2 %collective-permute-start.11 = (bf16[256,1024]{1,0:T(8,128)(2,1)S(1)}, bf16[256,1024]{1,0:T(8,128)(2,1)S(1)}, u32[]{:S(2)}, u32[]{:S(2)}) collective-permute-start(bf16[256,1024]{1,0:T(8,128)(2,1)S(1)} %collective-permute-done.7.refs_2_), channel_id=1, source_target_pairs={{8,0},{9,1},{10,2},{11,3},{12,4},{13,5},{14,6},{15,7}} | collective-permute-start | bytes 1572872 | tf_op jit(solution)/shard_map/ppermute | solution.py:234
  36.5 40.4 %copy-start.1 = (bf16[512,384]{1,0:T(8,128)(2,1)}, bf16[512,384]{1,0:T(8,128)(2,1)S(1)}, u32[]{:S(2)}) copy-start(bf16[512,384]{1,0:T(8,128)(2,1)S(1)} %pad_maximum_fusion.refs_7_) | copy-start | bytes 1179652
  36.5 9.1 %collective-permute-start.13 = (bf16[512,384]{1,0:T(8,128)(2,1)S(1)}, bf16[512,384]{1,0:T(8,128)(2,1)S(1)}, u32[]{:S(2)}, u32[]{:S(2)}) collective-permute-start(bf16[512,384]{1,0:T(8,128)(2,1)S(1)} %pad_maximum_fusion.refs_7_), channel_id=1, source_target_pairs={{0,2},{2,0},{4,6},{6,4},{1,3},{3,1},{5,7},{7,5},{8,10},{10,8},{12,... | collective-permute-start | bytes 1179656 | tf_op jit(solution)/shard_map/ppermute | solution.py:220
  45.6 12.7 %copy-start.15 = (bf16[512,384]{1,0:T(8,128)(2,1)}, bf16[512,384]{1,0:T(8,128)(2,1)S(1)}, u32[]{:S(2)}) copy-start(bf16[512,384]{1,0:T(8,128)(2,1)S(1)} %collective-permute-done.13.refs_8_) | copy-start | bytes 1179652
  45.6 9.7 %collective-permute-start.4 = (bf16[256,1024]{1,0:T(8,128)(2,1)S(1)}, bf16[256,1024]{1,0:T(8,128)(2,1)S(1)}, u32[]{:S(2)}, u32[]{:S(2)}) collective-permute-start(bf16[256,1024]{1,0:T(8,128)(2,1)S(1)} %collective-permute-done.3.refs_2_), channel_id=1, source_target_pairs={{0,1},{1,0},{8,9},{9,8},{16,17},{17,16},{2,3},{3,2},{10,11},{11,10... | collective-permute-start | bytes 1572872 | tf_op jit(solution)/shard_map/ppermute | solution.py:228
  47.5 9.3 %collective-permute-start.6 = (bf16[256,1024]{1,0:T(8,128)(2,1)S(1)}, bf16[256,1024]{1,0:T(8,128)(2,1)S(1)}, u32[]{:S(2)}, u32[]{:S(2)}) collective-permute-start(bf16[256,1024]{1,0:T(8,128)(2,1)S(1)} %collective-permute-done.5.refs_0_), channel_id=1, source_target_pairs={{16,17},{17,16},{24,25},{25,24},{18,19},{19,18},{26,27},{27,26},{2... | collective-permute-start | bytes 1572872 | tf_op jit(solution)/shard_map/ppermute | solution.py:228
  48.2 12.3 %copy-start.8 = (bf16[256,1024]{1,0:T(8,128)(2,1)}, bf16[256,1024]{1,0:T(8,128)(2,1)S(1)}, u32[]{:S(2)}) copy-start(bf16[256,1024]{1,0:T(8,128)(2,1)S(1)} %collective-permute-done.2.refs_1_) | copy-start | bytes 1572868
  48.2 10.1 %collective-permute-start.8 = (bf16[256,1024]{1,0:T(8,128)(2,1)S(1)}, bf16[256,1024]{1,0:T(8,128)(2,1)S(1)}, u32[]{:S(2)}, u32[]{:S(2)}) collective-permute-start(bf16[256,1024]{1,0:T(8,128)(2,1)S(1)} %collective-permute-done.7.refs_2_), channel_id=1, source_target_pairs={{0,1},{1,0},{8,9},{9,8},{2,3},{3,2},{10,11},{11,10},{4,5},{5,4},{1... | collective-permute-start | bytes 1572872 | tf_op jit(solution)/shard_map/ppermute | solution.py:228
  50.7 9.9 %copy-start.7 = (bf16[256,1024]{1,0:T(8,128)(2,1)}, bf16[256,1024]{1,0:T(8,128)(2,1)S(1)}, u32[]{:S(2)}) copy-start(bf16[256,1024]{1,0:T(8,128)(2,1)S(1)} %collective-permute-done.9.refs_0_) | copy-start | bytes 1572868
  50.7 8.6 %collective-permute-start.10 = (bf16[256,1024]{1,0:T(8,128)(2,1)S(1)}, bf16[256,1024]{1,0:T(8,128)(2,1)S(1)}, u32[]{:S(2)}, u32[]{:S(2)}) collective-permute-start(bf16[256,1024]{1,0:T(8,128)(2,1)S(1)} %collective-permute-done.9.refs_0_), channel_id=1, source_target_pairs={{24,25},{25,24},{26,27},{27,26},{28,29},{29,28},{30,31},{31,30}} | collective-permute-start | bytes 1572872 | tf_op jit(solution)/shard_map/ppermute | solution.py:228
  51.4 9.1 %copy-start.9 = (bf16[256,1024]{1,0:T(8,128)(2,1)}, bf16[256,1024]{1,0:T(8,128)(2,1)S(1)}, u32[]{:S(2)}) copy-start(bf16[256,1024]{1,0:T(8,128)(2,1)S(1)} %collective-permute-done.11.refs_2_) | copy-start | bytes 1572868
  51.4 9.1 %collective-permute-start.12 = (bf16[256,1024]{1,0:T(8,128)(2,1)S(1)}, bf16[256,1024]{1,0:T(8,128)(2,1)S(1)}, u32[]{:S(2)}, u32[]{:S(2)}) collective-permute-start(bf16[256,1024]{1,0:T(8,128)(2,1)S(1)} %collective-permute-done.11.refs_2_), channel_id=1, source_target_pairs={{0,1},{1,0},{2,3},{3,2},{4,5},{5,4},{6,7},{7,6}} | collective-permute-start | bytes 1572872 | tf_op jit(solution)/shard_map/ppermute | solution.py:228
  55.3 3.0 %copy-start.10 = (bf16[256,1024]{1,0:T(8,128)(2,1)}, bf16[256,1024]{1,0:T(8,128)(2,1)S(1)}, u32[]{:S(2)}) copy-start(bf16[256,1024]{1,0:T(8,128)(2,1)S(1)} %collective-permute-done.4.refs_3_) | copy-start | bytes 1572868
  55.3 21.6 %collective-permute-start.14 = (bf16[512,384]{1,0:T(8,128)(2,1)S(1)}, bf16[512,384]{1,0:T(8,128)(2,1)}, u32[]{:S(2)}, u32[]{:S(2)}) collective-permute-start(bf16[512,384]{1,0:T(8,128)(2,1)S(1)} %pad_maximum_fusion.refs_7_), channel_id=1, source_target_pairs={{0,4},{2,6},{4,0},{6,2},{1,5},{3,7},{5,1},{7,3},{8,12},{10,14},{12... | collective-permute-start | bytes 1179656 | tf_op jit(solution)/shard_map/ppermute | solution.py:220
  56.9 1.4 %copy-start.11 = (bf16[256,1024]{1,0:T(8,128)(2,1)}, bf16[256,1024]{1,0:T(8,128)(2,1)S(1)}, u32[]{:S(2)}) copy-start(bf16[256,1024]{1,0:T(8,128)(2,1)S(1)} %collective-permute-done.6.refs_1_) | copy-start | bytes 1572868
  56.9 20.0 %collective-permute-start.15 = (bf16[512,384]{1,0:T(8,128)(2,1)S(1)}, bf16[512,384]{1,0:T(8,128)(2,1)}, u32[]{:S(2)}, u32[]{:S(2)}) collective-permute-start(bf16[512,384]{1,0:T(8,128)(2,1)S(1)} %pad_maximum_fusion.refs_7_), channel_id=1, source_target_pairs={{0,6},{2,4},{4,2},{6,0},{1,7},{3,5},{5,3},{7,1},{8,14},{10,12},{12... | collective-permute-start | bytes 1179656 | tf_op jit(solution)/shard_map/ppermute | solution.py:220
  58.4 29.3 %copy-start.2 = (bf16[512,384]{1,0:T(8,128)(2,1)}, bf16[512,384]{1,0:T(8,128)(2,1)S(1)}, u32[]{:S(2)}) copy-start(bf16[512,384]{1,0:T(8,128)(2,1)S(1)} %pad_maximum_fusion.1.refs_7_) | copy-start | bytes 1179652
  58.4 2.2 %copy-start.12 = (bf16[256,1024]{1,0:T(8,128)(2,1)}, bf16[256,1024]{1,0:T(8,128)(2,1)S(1)}, u32[]{:S(2)}) copy-start(bf16[256,1024]{1,0:T(8,128)(2,1)S(1)} %collective-permute-done.8.refs_3_) | copy-start | bytes 1572868
  58.4 30.5 %collective-permute-start.20 = (bf16[512,384]{1,0:T(8,128)(2,1)S(1)}, bf16[512,384]{1,0:T(8,128)(2,1)}, u32[]{:S(2)}, u32[]{:S(2)}) collective-permute-start(bf16[512,384]{1,0:T(8,128)(2,1)S(1)} %pad_maximum_fusion.1.refs_7_), channel_id=1, source_target_pairs={{0,2},{2,0},{4,6},{6,4},{1,3},{3,1},{5,7},{7,5},{8,10},{10,8},{12,... | collective-permute-start | bytes 1179656 | tf_op jit(solution)/shard_map/ppermute | solution.py:220
  59.3 1.3 %copy-start.13 = (bf16[256,1024]{1,0:T(8,128)(2,1)}, bf16[256,1024]{1,0:T(8,128)(2,1)S(1)}, u32[]{:S(2)}) copy-start(bf16[256,1024]{1,0:T(8,128)(2,1)S(1)} %collective-permute-done.10.refs_1_) | copy-start | bytes 1572868
  59.3 32.9 %collective-permute-start.21 = (bf16[512,384]{1,0:T(8,128)(2,1)S(1)}, bf16[512,384]{1,0:T(8,128)(2,1)}, u32[]{:S(2)}, u32[]{:S(2)}) collective-permute-start(bf16[512,384]{1,0:T(8,128)(2,1)S(1)} %pad_maximum_fusion.1.refs_7_), channel_id=1, source_target_pairs={{0,4},{2,6},{4,0},{6,2},{1,5},{3,7},{5,1},{7,3},{8,12},{10,14},{12... | collective-permute-start | bytes 1179656 | tf_op jit(solution)/shard_map/ppermute | solution.py:220
  60.6 0.8 copy-start.14
  61.4 30.8 %collective-permute-start.22 = (bf16[512,384]{1,0:T(8,128)(2,1)S(1)}, bf16[512,384]{1,0:T(8,128)(2,1)}, u32[]{:S(2)}, u32[]{:S(2)}) collective-permute-start(bf16[512,384]{1,0:T(8,128)(2,1)S(1)} %pad_maximum_fusion.1.refs_7_), channel_id=1, source_target_pairs={{0,6},{2,4},{4,2},{6,0},{1,7},{3,5},{5,3},{7,1},{8,14},{10,12},{12... | collective-permute-start | bytes 1179656 | tf_op jit(solution)/shard_map/ppermute | solution.py:220
  87.7 14.7 %collective-permute-start.16 = (bf16[256,128]{1,0:T(8,128)(2,1)}, bf16[256,128]{1,0:T(8,128)(2,1)S(1)}, u32[]{:S(2)}, u32[]{:S(2)}) collective-permute-start(bf16[256,128]{1,0:T(8,128)(2,1)} %get-tuple-element.30), channel_id=1, source_target_pairs={{0,8},{8,16},{16,24},{24,0},{1,9},{9,17},{17,25},{25,1},{2,10},{10... | collective-permute-start | bytes 196616 | tf_op jit(solution)/shard_map/ppermute | solution.py:220
  88.9 16.2 %collective-permute-start.17 = (bf16[256,128]{1,0:T(8,128)(2,1)}, bf16[256,128]{1,0:T(8,128)(2,1)S(1)}, u32[]{:S(2)}, u32[]{:S(2)}) collective-permute-start(bf16[256,128]{1,0:T(8,128)(2,1)} %get-tuple-element.31), channel_id=1, source_target_pairs={{0,16},{8,24},{16,0},{24,8},{1,17},{9,25},{17,1},{25,9},{2,18},{10... | collective-permute-start | bytes 196616 | tf_op jit(solution)/shard_map/ppermute | solution.py:220
  88.9 16.2 %collective-permute-start.18 = (bf16[256,128]{1,0:T(8,128)(2,1)}, bf16[256,128]{1,0:T(8,128)(2,1)S(1)}, u32[]{:S(2)}, u32[]{:S(2)}) collective-permute-start(bf16[256,128]{1,0:T(8,128)(2,1)} %get-tuple-element.32), channel_id=1, source_target_pairs={{0,24},{8,0},{16,8},{24,16},{1,25},{9,1},{17,9},{25,17},{2,26},{10... | collective-permute-start | bytes 196616 | tf_op jit(solution)/shard_map/ppermute | solution.py:220
  100.8 7.0 %collective-permute-start.23 = (bf16[256,128]{1,0:T(8,128)(2,1)}, bf16[256,128]{1,0:T(8,128)(2,1)S(1)}, u32[]{:S(2)}, u32[]{:S(2)}) collective-permute-start(bf16[256,128]{1,0:T(8,128)(2,1)} %get-tuple-element.36), channel_id=1, source_target_pairs={{0,8},{8,16},{16,24},{24,0},{1,9},{9,17},{17,25},{25,1},{2,10},{10... | collective-permute-start | bytes 196616 | tf_op jit(solution)/shard_map/ppermute | solution.py:220
  101.5 7.7 %collective-permute-start.24 = (bf16[256,128]{1,0:T(8,128)(2,1)}, bf16[256,128]{1,0:T(8,128)(2,1)S(1)}, u32[]{:S(2)}, u32[]{:S(2)}) collective-permute-start(bf16[256,128]{1,0:T(8,128)(2,1)} %get-tuple-element.37), channel_id=1, source_target_pairs={{0,16},{8,24},{16,0},{24,8},{1,17},{9,25},{17,1},{25,9},{2,18},{10... | collective-permute-start | bytes 196616 | tf_op jit(solution)/shard_map/ppermute | solution.py:220
  102.4 2.7 %copy-start.18 = (bf16[256,128]{1,0:T(8,128)(2,1)}, bf16[256,128]{1,0:T(8,128)(2,1)S(1)}, u32[]{:S(2)}) copy-start(bf16[256,128]{1,0:T(8,128)(2,1)S(1)} %collective-permute-done.16.refs_1_) | copy-start | bytes 196612
  102.4 6.8 %collective-permute-start.25 = (bf16[256,128]{1,0:T(8,128)(2,1)}, bf16[256,128]{1,0:T(8,128)(2,1)S(1)}, u32[]{:S(2)}, u32[]{:S(2)}) collective-permute-start(bf16[256,128]{1,0:T(8,128)(2,1)} %get-tuple-element.38), channel_id=1, source_target_pairs={{0,24},{8,0},{16,8},{24,16},{1,25},{9,1},{17,9},{25,17},{2,26},{10... | collective-permute-start | bytes 196616 | tf_op jit(solution)/shard_map/ppermute | solution.py:220
  105.1 0.6 copy-start.20
  107.4 4.1 %collective-permute-start.19 = (bf16[128,512]{1,0:T(8,128)(2,1)}, bf16[128,512]{1,0:T(8,128)(2,1)S(1)}, u32[]{:S(2)}, u32[]{:S(2)}) collective-permute-start(bf16[128,512]{1,0:T(8,128)(2,1)} %get-tuple-element.34), channel_id=1, source_target_pairs={{0,1},{1,0},{2,3},{3,2},{4,5},{5,4},{6,7},{7,6},{8,9},{9,8},{10,11... | collective-permute-start | bytes 393224 | tf_op jit(solution)/shard_map/ppermute | solution.py:220
  107.8 1.5 %copy-start.21 = (bf16[256,128]{1,0:T(8,128)(2,1)}, bf16[256,128]{1,0:T(8,128)(2,1)S(1)}, u32[]{:S(2)}) copy-start(bf16[256,128]{1,0:T(8,128)(2,1)S(1)} %collective-permute-done.23.refs_1_) | copy-start | bytes 196612
  109.2 0.6 copy-start.23
  111.5 1.6 %collective-permute-start.26 = (bf16[128,512]{1,0:T(8,128)(2,1)}, bf16[128,512]{1,0:T(8,128)(2,1)S(1)}, u32[]{:S(2)}, u32[]{:S(2)}) collective-permute-start(bf16[128,512]{1,0:T(8,128)(2,1)} %get-tuple-element.40), channel_id=1, source_target_pairs={{0,1},{1,0},{2,3},{3,2},{4,5},{5,4},{6,7},{7,6},{8,9},{9,8},{10,11... | collective-permute-start | bytes 393224 | tf_op jit(solution)/shard_map/ppermute | solution.py:220
  111.5 1.6 %copy-start.16 = (bf16[128,512]{1,0:T(8,128)(2,1)}, bf16[128,512]{1,0:T(8,128)(2,1)S(1)}, u32[]{:S(2)}) copy-start(bf16[128,512]{1,0:T(8,128)(2,1)S(1)} %collective-permute-done.19.refs_1_) | copy-start | bytes 393220
  (3 other events, 1.9 us)
where the time goes:
time: 120 us; the launch traced here: 119 us
  Pallas kernels  40.8 us (34%)
  waiting for transfers between devices  35.6 us (30%)
  starting transfers between devices  35.5 us (30%)
  local copies, waits for them, and re-layouts  7.05 us (6%)
    pallas_call x9, Pallas kernels, call(): pl.pallas_call(kernel, out_shape=outs, in_specs=[smem] * len(scalars) + [...  40.8 us
    ppermute x14, starting transfers between devices, permuted(): lax.ppermute(x, axis, [(i, to(i)) for i in range(lax.axis_size(axis))])  16.8 us
    ppermute x3, waiting for transfers between devices, chain_blocks(): lax.ppermute(down, 'sp', [(i, i - 1) for i in range(1, size - k + 1)])  14.1 us
    ppermute x14, waiting for transfers between devices, permuted(): lax.ppermute(x, axis, [(i, to(i)) for i in range(lax.axis_size(axis))])  11.3 us
    ppermute x3, waiting for transfers between devices, chain_blocks(): up = lax.ppermute(up, 'sp', [(i, i + 1) for i in range(k - 1, size - 1)])  10.2 us
    ppermute x7, starting transfers between devices, swap(): return lax.ppermute(a, ('sp', 'tp'), pairs)  8.39 us
    ppermute x3, starting transfers between devices, chain_blocks(): up = lax.ppermute(up, 'sp', [(i, i + 1) for i in range(k - 1, size - 1)])  6.49 us
    ppermute x3, starting transfers between devices, chain_blocks(): lax.ppermute(down, 'sp', [(i, i - 1) for i in range(1, size - k + 1)])  3.85 us
  transfers between devices with their start and end apart: 27, of which 8 were waited for; matrix products, arithmetic and copies ran while one was open for 4% of the time, Pallas kernels for 29%

commit v1 on v0

--- a/solution.py
+++ b/solution.py
@@ -220,20 +220,24 @@
     return lax.ppermute(x, axis, [(i, to(i)) for i in range(lax.axis_size(axis))])
 
 
-def chain_blocks(x):
-    size, pair = lax.axis_size("sp"), lax.axis_size("tp")
-
-    def swap(a, valid):
-        pairs = [(s * pair + t, s * pair + 1 - t) for s in valid for t in range(pair)]
-        return lax.ppermute(a, ("sp", "tp"), pairs)
-
-    up = down = x
-    stages = [[(x, swap(x, range(size)), 0)]]
-    for k in range(1, size):
-        up = lax.ppermute(up, "sp", [(i, i + 1) for i in range(k - 1, size - 1)])
-        down = lax.ppermute(down, "sp", [(i, i - 1) for i in range(1, size - k + 1)])
-        from_up = (up, swap(up, range(k, size)), -k)
-        stages.append([from_up, (down, swap(down, range(size - k)), k)])
+def ring_blocks(x):
+    size = lax.axis_size("sp")
+
+    def pair(a, offset, row):
+        return (a, permuted(a, "tp", lambda i: 1 - i), offset, row)
+
+    def send(a, by):
+        return permuted(a, "sp", lambda i: (i + by) % size)
+
+    behind = ahead = x
+    stages = [[pair(x, 0, 0)]]
+    for k in range(1, (size - 1) // 2 + 1):
+        behind, ahead = send(behind, 1), send(ahead, -1)
+        stages.append([pair(behind, size - k, 0), pair(ahead, k, 0)])
+    if size % 2 == 0:
+        k, half = size // 2, x.shape[0] // 2
+        first, second = send(behind[:half], 1), send(ahead[half:], -1)
+        stages.append([pair(first, k, 0), pair(second, k, half)])
     return stages
 
 
@@ -255,48 +259,41 @@
 
 
 def normalize_stage(stage, gain):
-    rows, width = stage[0][0].shape
-    size = lax.axis_size("sp")
-    arrays = [a for own, other, _ in stage for a in (own, other)]
+    width = stage[0][0].shape[1]
+    arrays = [a for piece in stage for a in piece[:2]]
 
     def kernel(gain_ref, *refs):
         ins, outs = refs[: len(arrays)], refs[len(arrays) :]
-        sp_index, tp_index = lax.axis_index("sp"), lax.axis_index("tp")
-        for n, (_, _, offset) in enumerate(stage):
-            block = sp_index + offset
-
-            @pl.when((block >= 0) & (block < size))
-            def _():
-                a = ins[2 * n][...].astype(jnp.float32)
-                b = ins[2 * n + 1][...].astype(jnp.float32)
-                total = jnp.sum(a * a + b * b, axis=-1, keepdims=True)
-                scale = lax.rsqrt(total / (2 * width) + epsilon)
-                gain_a = gain_ref[pl.ds(tp_index, 1), :]
-                gain_b = gain_ref[pl.ds(1 - tp_index, 1), :]
-                outs[n][0] = (a * scale * gain_a).astype(jnp.bfloat16)
-                outs[n][1] = (b * scale * gain_b).astype(jnp.bfloat16)
-
-    out = [jax.ShapeDtypeStruct((2, rows, width), jnp.bfloat16)] * len(stage)
+        tp_index = lax.axis_index("tp")
+        gain_a = gain_ref[pl.ds(tp_index, 1), :]
+        gain_b = gain_ref[pl.ds(1 - tp_index, 1), :]
+        for n in range(len(stage)):
+            a = ins[2 * n][...].astype(jnp.float32)
+            b = ins[2 * n + 1][...].astype(jnp.float32)
+            total = jnp.sum(a * a + b * b, axis=-1, keepdims=True)
+            scale = lax.rsqrt(total / (2 * width) + epsilon)
+            outs[n][0] = (a * scale * gain_a).astype(jnp.bfloat16)
+            outs[n][1] = (b * scale * gain_b).astype(jnp.bfloat16)
+
+    out = [jax.ShapeDtypeStruct((2, *piece[0].shape), jnp.bfloat16) for piece in stage]
     normed = call(kernel, out, [], [], [gain.reshape(2, width)] + arrays)
-    return [(a, offset) for a, (_, _, offset) in zip(normed, stage)]
-
-
-def project(normed_refs, offsets, piece_refs, pieces, weight_ref, qkv_ref):
-    _, rows, width = normed_refs[0].shape
+    return [(a, *piece[2:]) for a, piece in zip(normed, stage)]
+
+
+def project(normed_refs, places, rows, piece_refs, pieces, weight_ref, qkv_ref):
+    width = normed_refs[0].shape[2]
     member_rows = pieces[0][0].shape[0]
     sp_index, fs_index, tp_index = (lax.axis_index(a) for a in ("sp", "fs", "tp"))
+    size = lax.axis_size("sp")
     for ref, (_, k) in zip(piece_refs, pieces):
         weight_ref[pl.ds((fs_index ^ k) * member_rows, member_rows), :] = ref[...]
-    for ref, offset in zip(normed_refs, offsets):
-        block = sp_index + offset
-
-        @pl.when((block >= 0) & (block * rows < qkv_ref.shape[0]))
-        def _():
-            own = weight_ref[pl.ds(tp_index * width, width), :]
-            other = weight_ref[pl.ds((1 - tp_index) * width, width), :]
-            result = jnp.dot(ref[0], own, preferred_element_type=jnp.float32)
-            result += jnp.dot(ref[1], other, preferred_element_type=jnp.float32)
-            qkv_ref[pl.ds(block * rows, rows), :] = result.astype(jnp.bfloat16)
+    own = weight_ref[pl.ds(tp_index * width, width), :]
+    other = weight_ref[pl.ds((1 - tp_index) * width, width), :]
+    for ref, (offset, row) in zip(normed_refs, places):
+        result = jnp.dot(ref[0], own, preferred_element_type=jnp.float32)
+        result += jnp.dot(ref[1], other, preferred_element_type=jnp.float32)
+        start = lax.rem(sp_index + offset, size) * rows + row
+        qkv_ref[pl.ds(start, ref.shape[1]), :] = result.astype(jnp.bfloat16)
 
 
 def mix_head(kernel_of, scalars, gain, normed, pieces):
@@ -304,13 +301,13 @@
     size = lax.axis_size("sp")
     columns = pieces[0][0].shape[1]
     head_width = gain.shape[0] // size
-    offsets = [offset for _, offset in normed]
+    places = [piece[1:] for piece in normed]
 
     def kernel(scalar_ref, gain_ref, *refs):
         normed_refs, refs = refs[: len(normed)], refs[len(normed) :]
         piece_refs, refs = refs[: len(pieces)], refs[len(pieces) :]
         out_refs, (weight_ref, qkv_ref, mixed_ref) = refs[:size], refs[size:]
-        project(normed_refs, offsets, piece_refs, pieces, weight_ref, qkv_ref)
+        project(normed_refs, places, rows, piece_refs, pieces, weight_ref, qkv_ref)
         sp_index = lax.axis_index("sp")
 
         def store(block, value):
@@ -331,7 +328,7 @@
             pltpu.VMEM((length, head_width), jnp.bfloat16),
         ],
         [scalars],
-        [gain.reshape(size, head_width)] + [a for a, _ in normed] + [p[0] for p in pieces],
+        [gain.reshape(size, head_width)] + [p[0] for p in normed + pieces],
     )
 
 
@@ -499,7 +496,7 @@
 
     att_own = head_columns(query_weight, key_weight, value_weight)
     ret_own = head_columns(state_query, state_key, state_value)
-    stages = chain_blocks(tokens[0])
+    stages = ring_blocks(tokens[0])
     att_pieces = cube_pieces(att_own, "fs")
     ret_pieces = cube_pieces(ret_own, "fs")
     normed = []

time: 120 us -> 106 us (0.88)
  starting transfers between devices: 35.5 us -> 25.9 us
  Pallas kernels: 40.8 us -> 33.8 us
  waiting for transfers between devices: 35.6 us -> 39 us
    ppermute x14 -> x23, waiting for transfers between devices: 11.3 us -> 39 us  [permuted(): lax.ppermute(x, axis, [(i, to(i)) for i in range(lax.axis_size(axis))])]
    ppermute x13 -> x0, waiting for transfers between devices: 24.2 us -> none  [the longest x3 14.1 us: chain_blocks(): lax.ppermute(down, 'sp', [(i, i - 1) for i in range(1, size - k + 1)])]
    ppermute x13 -> x0, starting transfers between devices: 18.7 us -> none  [the longest x7 8.39 us: swap(): return lax.ppermute(a, ('sp', 'tp'), pairs)]
    ppermute x14 -> x23, starting transfers between devices: 16.8 us -> 25.9 us  [permuted(): lax.ppermute(x, axis, [(i, to(i)) for i in range(lax.axis_size(axis))])]
    pallas_call x9 -> x8, Pallas kernels: 40.8 us -> 33.8 us  [call(): pl.pallas_call(kernel, out_shape=outs, in_specs=[smem] * len(scalars) + [...]
    unnamed x48 -> x42, local copies, waits for them, and re-layouts: 2.81 us -> 2.67 us
  transfers between devices with their start and end apart: 27 -> 23, of which waited for: 8 -> 9; matrix products, arithmetic and copies ran while one was open for 4% -> 4% of each run, Pallas kernels for 29% -> 26%
where the time goes in v1:
time: 106 us
  waiting for transfers between devices  39 us (37%)
  Pallas kernels  33.8 us (32%)
  starting transfers between devices  25.9 us (24%)
  local copies, waits for them, and re-layouts  7.02 us (7%)
    ppermute x23, waiting for transfers between devices, permuted(): lax.ppermute(x, axis, [(i, to(i)) for i in range(lax.axis_size(axis))])  39 us
    pallas_call x8, Pallas kernels, call(): pl.pallas_call(kernel, out_shape=outs, in_specs=[smem] * len(scalars) + [...  33.8 us
    ppermute x23, starting transfers between devices, permuted(): lax.ppermute(x, axis, [(i, to(i)) for i in range(lax.axis_size(axis))])  25.9 us
    dynamic_slice x4, local copies, waits for them, and re-layouts, head_columns(): lax.dynamic_slice_in_dim(w, sp_index * each, each, 1)  3.02 us
    unnamed x42, local copies, waits for them, and re-layouts  2.67 us
  transfers between devices with their start and end apart: 23, of which 9 were waited for; matrix products, arithmetic and copies ran while one was open for 4% of the time, Pallas kernels for 26%

profile of v1, /device:TPU:0, one launch (start us, length us, event | category | flops | bytes accessed | tf_op | source)
XLA Modules:
  0.0 106.1 jit_solution(11162519997268985414)
XLA Ops:
  0.0 3.1 %collective-permute-start.1 = (bf16[256,1024]{1,0:T(8,128)(2,1)}, bf16[256,1024]{1,0:T(8,128)(2,1)S(1)}, u32[]{:S(2)}, u32[]{:S(2)}) collective-permute-start(bf16[256,1024]{1,0:T(8,128)(2,1)} %bitcast.4), channel_id=1, source_target_pairs={{0,8},{8,16},{16,24},{24,0},{1,9},{9,17},{17,25},{25,1},{2,10},{10... | collective-permute-start | bytes 1572872 | tf_op jit(solution)/shard_map/ppermute | solution.py:220
  3.1 2.1 %collective-permute-start.3 = (bf16[256,1024]{1,0:T(8,128)(2,1)}, bf16[256,1024]{1,0:T(8,128)(2,1)S(1)}, u32[]{:S(2)}, u32[]{:S(2)}) collective-permute-start(bf16[256,1024]{1,0:T(8,128)(2,1)} %bitcast.5), channel_id=1, source_target_pairs={{0,24},{8,0},{16,8},{24,16},{1,25},{9,1},{17,9},{25,17},{2,26},{10... | collective-permute-start | bytes 1572872 | tf_op jit(solution)/shard_map/ppermute | solution.py:220
  5.1 1.0 constant_dynamic-slice_fusion.3
  6.2 0.1 pad_maximum_fusion.refs_5_
  6.2 1.7 %collective-permute-start.9 = (bf16[512,384]{1,0:T(8,128)(2,1)S(1)}, bf16[512,384]{1,0:T(8,128)(2,1)S(1)}, u32[]{:S(2)}, u32[]{:S(2)}) collective-permute-start(bf16[512,384]{1,0:T(8,128)(2,1)S(1)} %pad_maximum_fusion.refs_5_), channel_id=1, source_target_pairs={{0,2},{2,0},{4,6},{6,4},{1,3},{3,1},{5,7},{7,5},{8,10},{10,8},{12,... | collective-permute-start | bytes 1179656 | tf_op jit(solution)/shard_map/ppermute | solution.py:220
  8.0 10.1 %collective-permute-done.1.refs_0_ = bf16[256,1024]{1,0:T(8,128)(2,1)S(1)} collective-permute-done((bf16[256,1024]{1,0:T(8,128)(2,1)}, bf16[256,1024]{1,0:T(8,128)(2,1)S(1)}, u32[]{:S(2)}, u32[]{:S(2)}) %collective-permute-start.1) | collective-permute-done | bytes 524320 | tf_op jit(solution)/shard_map/ppermute | solution.py:220
  18.1 0.0 collective-permute-start.2
  18.1 0.1 collective-permute-start.5
  18.2 9.7 %collective-permute-done.3.refs_2_ = bf16[256,1024]{1,0:T(8,128)(2,1)S(1)} collective-permute-done((bf16[256,1024]{1,0:T(8,128)(2,1)}, bf16[256,1024]{1,0:T(8,128)(2,1)S(1)}, u32[]{:S(2)}, u32[]{:S(2)}) %collective-permute-start.3) | collective-permute-done | bytes 524320 | tf_op jit(solution)/shard_map/ppermute | solution.py:220
  27.9 3.3 %collective-permute-start.7 = (bf16[128,1024]{1,0:T(8,128)(2,1)S(1)}, bf16[128,1024]{1,0:T(8,128)(2,1)S(1)}, u32[]{:S(2)}, u32[]{:S(2)}) collective-permute-start(bf16[128,1024]{1,0:T(8,128)(2,1)S(1)} %slice.9), channel_id=1, source_target_pairs={{0,24},{8,0},{16,8},{24,16},{1,25},{9,1},{17,9},{25,17},{2,26},{10... | collective-permute-start | bytes 786440 | tf_op jit(solution)/shard_map/ppermute | solution.py:220
  31.2 0.0 collective-permute-done.9.refs_6_
  31.2 5.3 %collective-permute-done.5.refs_0_ = bf16[128,1024]{1,0:T(8,128)(2,1)S(1)} collective-permute-done((bf16[128,1024]{1,0:T(8,128)(2,1)S(1)}, bf16[128,1024]{1,0:T(8,128)(2,1)S(1)}, u32[]{:S(2)}, u32[]{:S(2)}) %collective-permute-start.5) | collective-permute-done | bytes 262176 | tf_op jit(solution)/shard_map/ppermute | solution.py:220
  36.5 4.7 %collective-permute-done.7.refs_2_ = bf16[128,1024]{1,0:T(8,128)(2,1)S(1)} collective-permute-done((bf16[128,1024]{1,0:T(8,128)(2,1)S(1)}, bf16[128,1024]{1,0:T(8,128)(2,1)S(1)}, u32[]{:S(2)}, u32[]{:S(2)}) %collective-permute-start.7) | collective-permute-done | bytes 262176 | tf_op jit(solution)/shard_map/ppermute | solution.py:220
  41.2 1.0 constant_dynamic-slice_fusion.2
  42.3 1.0 constant_dynamic-slice_fusion
  43.3 0.0 copy-start.5
  43.3 1.6 %collective-permute-start.10 = (bf16[512,384]{1,0:T(8,128)(2,1)S(1)}, bf16[512,384]{1,0:T(8,128)(2,1)}, u32[]{:S(2)}, u32[]{:S(2)}) collective-permute-start(bf16[512,384]{1,0:T(8,128)(2,1)S(1)} %pad_maximum_fusion.refs_5_), channel_id=1, source_target_pairs={{0,4},{2,6},{4,0},{6,2},{1,5},{3,7},{5,1},{7,3},{8,12},{10,14},{12... | collective-permute-start | bytes 1179656 | tf_op jit(solution)/shard_map/ppermute | solution.py:220
  44.9 1.4 %collective-permute-start.11 = (bf16[512,384]{1,0:T(8,128)(2,1)S(1)}, bf16[512,384]{1,0:T(8,128)(2,1)}, u32[]{:S(2)}, u32[]{:S(2)}) collective-permute-start(bf16[512,384]{1,0:T(8,128)(2,1)S(1)} %pad_maximum_fusion.refs_5_), channel_id=1, source_target_pairs={{0,6},{2,4},{4,2},{6,0},{1,7},{3,5},{5,3},{7,1},{8,14},{10,12},{12... | collective-permute-start | bytes 1179656 | tf_op jit(solution)/shard_map/ppermute | solution.py:220
  46.3 0.1 pad_maximum_fusion.1.refs_5_
  46.4 0.6 collective-permute-start.16
  47.0 1.5 %collective-permute-start.17 = (bf16[512,384]{1,0:T(8,128)(2,1)S(1)}, bf16[512,384]{1,0:T(8,128)(2,1)}, u32[]{:S(2)}, u32[]{:S(2)}) collective-permute-start(bf16[512,384]{1,0:T(8,128)(2,1)S(1)} %pad_maximum_fusion.1.refs_5_), channel_id=1, source_target_pairs={{0,4},{2,6},{4,0},{6,2},{1,5},{3,7},{5,1},{7,3},{8,12},{10,14},{12... | collective-permute-start | bytes 1179656 | tf_op jit(solution)/shard_map/ppermute | solution.py:220
  48.6 0.7 copy-done.12
  49.3 1.6 %collective-permute-start.18 = (bf16[512,384]{1,0:T(8,128)(2,1)S(1)}, bf16[512,384]{1,0:T(8,128)(2,1)}, u32[]{:S(2)}, u32[]{:S(2)}) collective-permute-start(bf16[512,384]{1,0:T(8,128)(2,1)S(1)} %pad_maximum_fusion.1.refs_5_), channel_id=1, source_target_pairs={{0,6},{2,4},{4,2},{6,0},{1,7},{3,5},{5,3},{7,1},{8,14},{10,12},{12... | collective-permute-start | bytes 1179656 | tf_op jit(solution)/shard_map/ppermute | solution.py:220
  50.9 1.3 %reshape.12.gain_ref = f32[2,1024]{1,0:T(2,128)} reshape(f32[2048]{0:T(1024)} %param.14) | data formatting | bytes 16384 | tf_op jit(solution)/shard_map/reshape | solution.py:279
  52.2 2.6 %shard_map.127.refs_0_ = bf16[2,256,1024]{2,1,0:T(8,128)(2,1)} custom-call(f32[2,1024]{1,0:T(2,128)} %reshape.12.gain_ref, bf16[256,1024]{1,0:T(8,128)(2,1)} %bitcast.7, bf16[256,1024]{1,0:T(8,128)(2,1)} %copy-done.5), custom_call_target="tpu_custom_call" | custom-call | tf_op jit(solution)/shard_map/pallas_call | solution.py:252
  54.8 3.5 %shard_map.128 = (bf16[2,256,1024]{2,1,0:T(8,128)(2,1)}, bf16[2,256,1024]{2,1,0:T(8,128)(2,1)}) custom-call(f32[2,1024]{1,0:T(2,128)} %reshape.12.gain_ref, bf16[256,1024]{1,0:T(8,128)(2,1)} %copy-done.3, bf16[256,1024]{1,0:T(8,128)(2,1)} %copy-done.6, bf16[256,1024]{1,0:T(8,128)(2,1)} %copy-done.4, bf16[256,1024]{1,0:T(8,128)(2,1)} %copy-done.7), custom_call_target="tpu_custom_call" | custom-call | tf_op jit(solution)/shard_map/pallas_call | solution.py:252
  58.2 2.5 %shard_map.129 = (bf16[2,128,1024]{2,1,0:T(8,128)(2,1)}, bf16[2,128,1024]{2,1,0:T(8,128)(2,1)}) custom-call(f32[2,1024]{1,0:T(2,128)} %reshape.12.gain_ref, bf16[128,1024]{1,0:T(8,128)(2,1)} %copy-done.9, bf16[128,1024]{1,0:T(8,128)(2,1)} %copy-done.11, bf16[128,1024]{1,0:T(8,128)(2,1)} %copy-done.10, bf16[128,1024]{1,0:T(8,128)(2,1)} %copy-done.12), custom_call_target="tpu_custom_call" | custom-call | tf_op jit(solution)/shard_map/pallas_call | solution.py:252
  60.7 3.1 %collective-permute-done.10.refs_7_ = bf16[512,384]{1,0:T(8,128)(2,1)} collective-permute-done((bf16[512,384]{1,0:T(8,128)(2,1)S(1)}, bf16[512,384]{1,0:T(8,128)(2,1)}, u32[]{:S(2)}, u32[]{:S(2)}) %collective-permute-start.10) | collective-permute-done | bytes 393248 | tf_op jit(solution)/shard_map/ppermute | solution.py:220
  63.9 9.0 %shard_map.130 = (bf16[256,128]{1,0:T(8,128)(2,1)}, bf16[256,128]{1,0:T(8,128)(2,1)}, bf16[256,128]{1,0:T(8,128)(2,1)}, bf16[256,128]{1,0:T(8,128)(2,1)}) custom-call(f32[4]{0:T(128)} %scalar_ref.2, f32[4,128]{1,0:T(4,128)} %bitcast.8, bf16[2,256,1024]{2,1,0:T(8,128)(2,1)} %shard_map.127.refs_0_, bf16[2,256,1024]{2,1,0:T(8,128)(2,1)} %get-tuple-element.21.refs_1_, ...), custom_call_target="tpu_custom_call" | custom-call | tf_op jit(solution)/shard_map/pallas_call | solution.py:252
  72.9 1.3 %collective-permute-start.12 = (bf16[256,128]{1,0:T(8,128)(2,1)}, bf16[256,128]{1,0:T(8,128)(2,1)S(1)}, u32[]{:S(2)}, u32[]{:S(2)}) collective-permute-start(bf16[256,128]{1,0:T(8,128)(2,1)} %get-tuple-element.26), channel_id=1, source_target_pairs={{0,8},{8,16},{16,24},{24,0},{1,9},{9,17},{17,25},{25,1},{2,10},{10... | collective-permute-start | bytes 196616 | tf_op jit(solution)/shard_map/ppermute | solution.py:220
  74.2 2.1 %collective-permute-start.13 = (bf16[256,128]{1,0:T(8,128)(2,1)}, bf16[256,128]{1,0:T(8,128)(2,1)S(1)}, u32[]{:S(2)}, u32[]{:S(2)}) collective-permute-start(bf16[256,128]{1,0:T(8,128)(2,1)} %get-tuple-element.27), channel_id=1, source_target_pairs={{0,16},{8,24},{16,0},{24,8},{1,17},{9,25},{17,1},{25,9},{2,18},{10... | collective-permute-start | bytes 196616 | tf_op jit(solution)/shard_map/ppermute | solution.py:220
  76.3 1.2 %collective-permute-start.14 = (bf16[256,128]{1,0:T(8,128)(2,1)}, bf16[256,128]{1,0:T(8,128)(2,1)S(1)}, u32[]{:S(2)}, u32[]{:S(2)}) collective-permute-start(bf16[256,128]{1,0:T(8,128)(2,1)} %get-tuple-element.28), channel_id=1, source_target_pairs={{0,24},{8,0},{16,8},{24,16},{1,25},{9,1},{17,9},{25,17},{2,26},{10... | collective-permute-start | bytes 196616 | tf_op jit(solution)/shard_map/ppermute | solution.py:220
  77.6 2.6 %collective-permute-done.17.refs_7_ = bf16[512,384]{1,0:T(8,128)(2,1)} collective-permute-done((bf16[512,384]{1,0:T(8,128)(2,1)S(1)}, bf16[512,384]{1,0:T(8,128)(2,1)}, u32[]{:S(2)}, u32[]{:S(2)}) %collective-permute-start.17) | collective-permute-done | bytes 393248 | tf_op jit(solution)/shard_map/ppermute | solution.py:220
  80.2 7.1 %shard_map.132 = (bf16[256,128]{1,0:T(8,128)(2,1)}, bf16[256,128]{1,0:T(8,128)(2,1)}, bf16[256,128]{1,0:T(8,128)(2,1)}, bf16[256,128]{1,0:T(8,128)(2,1)}) custom-call(f32[4]{0:T(128)} %scalar_ref.3, f32[4,128]{1,0:T(4,128)} %bitcast.9, bf16[2,256,1024]{2,1,0:T(8,128)(2,1)} %shard_map.127.refs_0_, bf16[2,256,1024]{2,1,0:T(8,128)(2,1)} %get-tuple-element.21.refs_1_, ...), custom_call_target="tpu_custom_call" | custom-call | tf_op jit(solution)/shard_map/pallas_call | solution.py:252
  87.3 1.2 %collective-permute-start.19 = (bf16[256,128]{1,0:T(8,128)(2,1)}, bf16[256,128]{1,0:T(8,128)(2,1)S(1)}, u32[]{:S(2)}, u32[]{:S(2)}) collective-permute-start(bf16[256,128]{1,0:T(8,128)(2,1)} %get-tuple-element.32), channel_id=1, source_target_pairs={{0,8},{8,16},{16,24},{24,0},{1,9},{9,17},{17,25},{25,1},{2,10},{10... | collective-permute-start | bytes 196616 | tf_op jit(solution)/shard_map/ppermute | solution.py:220
  88.5 1.9 %collective-permute-start.20 = (bf16[256,128]{1,0:T(8,128)(2,1)}, bf16[256,128]{1,0:T(8,128)(2,1)S(1)}, u32[]{:S(2)}, u32[]{:S(2)}) collective-permute-start(bf16[256,128]{1,0:T(8,128)(2,1)} %get-tuple-element.33), channel_id=1, source_target_pairs={{0,16},{8,24},{16,0},{24,8},{1,17},{9,25},{17,1},{25,9},{2,18},{10... | collective-permute-start | bytes 196616 | tf_op jit(solution)/shard_map/ppermute | solution.py:220
  90.3 1.2 %collective-permute-start.21 = (bf16[256,128]{1,0:T(8,128)(2,1)}, bf16[256,128]{1,0:T(8,128)(2,1)S(1)}, u32[]{:S(2)}, u32[]{:S(2)}) collective-permute-start(bf16[256,128]{1,0:T(8,128)(2,1)} %get-tuple-element.34), channel_id=1, source_target_pairs={{0,24},{8,0},{16,8},{24,16},{1,25},{9,1},{17,9},{25,17},{2,26},{10... | collective-permute-start | bytes 196616 | tf_op jit(solution)/shard_map/ppermute | solution.py:220
  91.6 0.6 copy-done.16
  92.2 0.0 copy-done.17
  92.2 1.7 %shard_map.131 = (bf16[128,512]{1,0:T(8,128)(2,1)}, bf16[128,512]{1,0:T(8,128)(2,1)}) custom-call(bf16[256,128]{1,0:T(8,128)(2,1)} %get-tuple-element.25.refs_0_, bf16[256,128]{1,0:T(8,128)(2,1)} %copy-done.15, bf16[256,128]{1,0:T(8,128)(2,1)} %copy-done.16, bf16[256,128]{1,0:T(8,128)(2,1)} %copy-done.17), custom_call_target="tpu_custom_call" | custom-call | tf_op jit(solution)/shard_map/pallas_call | solution.py:252
  93.9 0.3 collective-permute-done.19.refs_1_
  94.2 1.6 %collective-permute-done.20.refs_2_ = bf16[256,128]{1,0:T(8,128)(2,1)S(1)} collective-permute-done((bf16[256,128]{1,0:T(8,128)(2,1)}, bf16[256,128]{1,0:T(8,128)(2,1)S(1)}, u32[]{:S(2)}, u32[]{:S(2)}) %collective-permute-start.20) | collective-permute-done | bytes 65568 | tf_op jit(solution)/shard_map/ppermute | solution.py:220
  95.8 0.6 copy-done.19
  96.4 0.0 copy-done.20
  96.4 1.7 %shard_map.133 = (bf16[128,512]{1,0:T(8,128)(2,1)}, bf16[128,512]{1,0:T(8,128)(2,1)}) custom-call(bf16[256,128]{1,0:T(8,128)(2,1)} %get-tuple-element.31.refs_0_, bf16[256,128]{1,0:T(8,128)(2,1)} %copy-done.18, bf16[256,128]{1,0:T(8,128)(2,1)} %copy-done.19, bf16[256,128]{1,0:T(8,128)(2,1)} %copy-done.20), custom_call_target="tpu_custom_call" | custom-call | tf_op jit(solution)/shard_map/pallas_call | solution.py:252
  98.1 1.5 %collective-permute-done.22.refs_3_ = bf16[128,512]{1,0:T(8,128)(2,1)S(1)} collective-permute-done((bf16[128,512]{1,0:T(8,128)(2,1)}, bf16[128,512]{1,0:T(8,128)(2,1)S(1)}, u32[]{:S(2)}, u32[]{:S(2)}) %collective-permute-start.22) | collective-permute-done | bytes 131104 | tf_op jit(solution)/shard_map/ppermute | solution.py:220
  99.7 0.6 copy-done.14
  100.3 5.7 %shard_map.134 = bf16[128,2048]{1,0:T(8,128)(2,1)} custom-call(bf16[2048,2048]{1,0:T(8,128)(2,1)} %weight_ref.1, bf16[128,512]{1,0:T(8,128)(2,1)} %get-tuple-element.29.refs_0_, bf16[128,512]{1,0:T(8,128)(2,1)} %copy-done.13, bf16[128,512]{1,0:T(8,128)(2,1)} %get-tuple-element.35.refs_2_, bf16[128,512]{1,0:T(8,128)(2,1)} %copy-done.14), custom_call_target="tpu_custom_call" | custom-call | tf_op jit(solution)/shard_map/pallas_call | solution.py:252
  (57 shorter events, 0.2 us)
Async XLA Ops:
  0.0 6.1 %copy-start = (bf16[512,512]{1,0:T(8,128)(2,1)S(1)}, bf16[512,512]{1,0:T(8,128)(2,1)}, u32[]{:S(2)}) copy-start(bf16[512,512]{1,0:T(8,128)(2,1)} %param.15) | copy-start | bytes 1572868
  0.0 18.1 %collective-permute-start.1 = (bf16[256,1024]{1,0:T(8,128)(2,1)}, bf16[256,1024]{1,0:T(8,128)(2,1)S(1)}, u32[]{:S(2)}, u32[]{:S(2)}) collective-permute-start(bf16[256,1024]{1,0:T(8,128)(2,1)} %bitcast.4), channel_id=1, source_target_pairs={{0,8},{8,16},{16,24},{24,0},{1,9},{9,17},{17,25},{25,1},{2,10},{10... | collective-permute-start | bytes 1572872 | tf_op jit(solution)/shard_map/ppermute | solution.py:220
  3.1 24.8 %collective-permute-start.3 = (bf16[256,1024]{1,0:T(8,128)(2,1)}, bf16[256,1024]{1,0:T(8,128)(2,1)S(1)}, u32[]{:S(2)}, u32[]{:S(2)}) collective-permute-start(bf16[256,1024]{1,0:T(8,128)(2,1)} %bitcast.5), channel_id=1, source_target_pairs={{0,24},{8,0},{16,8},{24,16},{1,25},{9,1},{17,9},{25,17},{2,26},{10... | collective-permute-start | bytes 1572872 | tf_op jit(solution)/shard_map/ppermute | solution.py:220
  6.2 57.6 %copy-start.1 = (bf16[512,384]{1,0:T(8,128)(2,1)}, bf16[512,384]{1,0:T(8,128)(2,1)S(1)}, u32[]{:S(2)}) copy-start(bf16[512,384]{1,0:T(8,128)(2,1)S(1)} %pad_maximum_fusion.refs_5_) | copy-start | bytes 1179652
  6.2 25.0 %collective-permute-start.9 = (bf16[512,384]{1,0:T(8,128)(2,1)S(1)}, bf16[512,384]{1,0:T(8,128)(2,1)S(1)}, u32[]{:S(2)}, u32[]{:S(2)}) collective-permute-start(bf16[512,384]{1,0:T(8,128)(2,1)S(1)} %pad_maximum_fusion.refs_5_), channel_id=1, source_target_pairs={{0,2},{2,0},{4,6},{6,4},{1,3},{3,1},{5,7},{7,5},{8,10},{10,8},{12,... | collective-permute-start | bytes 1179656 | tf_op jit(solution)/shard_map/ppermute | solution.py:220
  8.0 35.3 %collective-permute-start = (bf16[256,1024]{1,0:T(8,128)(2,1)}, bf16[256,1024]{1,0:T(8,128)(2,1)S(1)}, u32[]{:S(2)}, u32[]{:S(2)}) collective-permute-start(bf16[256,1024]{1,0:T(8,128)(2,1)} %bitcast.6), channel_id=1, source_target_pairs={{0,1},{1,0},{2,3},{3,2},{4,5},{5,4},{6,7},{7,6},{8,9},{9,8},{10,11... | collective-permute-start | bytes 1572872 | tf_op jit(solution)/shard_map/ppermute | solution.py:220
  18.1 36.7 %copy-start.3 = (bf16[256,1024]{1,0:T(8,128)(2,1)}, bf16[256,1024]{1,0:T(8,128)(2,1)S(1)}, u32[]{:S(2)}) copy-start(bf16[256,1024]{1,0:T(8,128)(2,1)S(1)} %collective-permute-done.1.refs_0_) | copy-start | bytes 1572868
  18.1 26.8 %collective-permute-start.2 = (bf16[256,1024]{1,0:T(8,128)(2,1)S(1)}, bf16[256,1024]{1,0:T(8,128)(2,1)S(1)}, u32[]{:S(2)}, u32[]{:S(2)}) collective-permute-start(bf16[256,1024]{1,0:T(8,128)(2,1)S(1)} %collective-permute-done.1.refs_0_), channel_id=1, source_target_pairs={{0,1},{1,0},{2,3},{3,2},{4,5},{5,4},{6,7},{7,6},{8,9},{9,8},{10,11... | collective-permute-start | bytes 1572872 | tf_op jit(solution)/shard_map/ppermute | solution.py:220
  18.1 18.4 %collective-permute-start.5 = (bf16[128,1024]{1,0:T(8,128)(2,1)S(1)}, bf16[128,1024]{1,0:T(8,128)(2,1)S(1)}, u32[]{:S(2)}, u32[]{:S(2)}) collective-permute-start(bf16[128,1024]{1,0:T(8,128)(2,1)S(1)} %slice.8), channel_id=1, source_target_pairs={{0,8},{8,16},{16,24},{24,0},{1,9},{9,17},{17,25},{25,1},{2,10},{10... | collective-permute-start | bytes 786440 | tf_op jit(solution)/shard_map/ppermute | solution.py:220
  27.9 26.9 %copy-start.4 = (bf16[256,1024]{1,0:T(8,128)(2,1)}, bf16[256,1024]{1,0:T(8,128)(2,1)S(1)}, u32[]{:S(2)}) copy-start(bf16[256,1024]{1,0:T(8,128)(2,1)S(1)} %collective-permute-done.3.refs_2_) | copy-start | bytes 1572868
  27.9 13.3 %collective-permute-start.7 = (bf16[128,1024]{1,0:T(8,128)(2,1)S(1)}, bf16[128,1024]{1,0:T(8,128)(2,1)S(1)}, u32[]{:S(2)}, u32[]{:S(2)}) collective-permute-start(bf16[128,1024]{1,0:T(8,128)(2,1)S(1)} %slice.9), channel_id=1, source_target_pairs={{0,24},{8,0},{16,8},{24,16},{1,25},{9,1},{17,9},{25,17},{2,26},{10... | collective-permute-start | bytes 786440 | tf_op jit(solution)/shard_map/ppermute | solution.py:220
  31.2 15.1 %copy-start.8 = (bf16[512,384]{1,0:T(8,128)(2,1)}, bf16[512,384]{1,0:T(8,128)(2,1)S(1)}, u32[]{:S(2)}) copy-start(bf16[512,384]{1,0:T(8,128)(2,1)S(1)} %collective-permute-done.9.refs_6_) | copy-start | bytes 1179652
  31.2 15.2 %collective-permute-start.4 = (bf16[256,1024]{1,0:T(8,128)(2,1)S(1)}, bf16[256,1024]{1,0:T(8,128)(2,1)S(1)}, u32[]{:S(2)}, u32[]{:S(2)}) collective-permute-start(bf16[256,1024]{1,0:T(8,128)(2,1)S(1)} %collective-permute-done.3.refs_2_), channel_id=1, source_target_pairs={{0,1},{1,0},{2,3},{3,2},{4,5},{5,4},{6,7},{7,6},{8,9},{9,8},{10,11... | collective-permute-start | bytes 1572872 | tf_op jit(solution)/shard_map/ppermute | solution.py:220
  36.5 12.0 %copy-start.9 = (bf16[128,1024]{1,0:T(8,128)(2,1)}, bf16[128,1024]{1,0:T(8,128)(2,1)S(1)}, u32[]{:S(2)}) copy-start(bf16[128,1024]{1,0:T(8,128)(2,1)S(1)} %collective-permute-done.5.refs_0_) | copy-start | bytes 786436
  36.5 10.5 %collective-permute-start.6 = (bf16[128,1024]{1,0:T(8,128)(2,1)S(1)}, bf16[128,1024]{1,0:T(8,128)(2,1)S(1)}, u32[]{:S(2)}, u32[]{:S(2)}) collective-permute-start(bf16[128,1024]{1,0:T(8,128)(2,1)S(1)} %collective-permute-done.5.refs_0_), channel_id=1, source_target_pairs={{0,1},{1,0},{2,3},{3,2},{4,5},{5,4},{6,7},{7,6},{8,9},{9,8},{10,11... | collective-permute-start | bytes 786440 | tf_op jit(solution)/shard_map/ppermute | solution.py:220
  41.2 7.3 %copy-start.10 = (bf16[128,1024]{1,0:T(8,128)(2,1)}, bf16[128,1024]{1,0:T(8,128)(2,1)S(1)}, u32[]{:S(2)}) copy-start(bf16[128,1024]{1,0:T(8,128)(2,1)S(1)} %collective-permute-done.7.refs_2_) | copy-start | bytes 786436
  41.2 7.3 %collective-permute-start.8 = (bf16[128,1024]{1,0:T(8,128)(2,1)S(1)}, bf16[128,1024]{1,0:T(8,128)(2,1)S(1)}, u32[]{:S(2)}, u32[]{:S(2)}) collective-permute-start(bf16[128,1024]{1,0:T(8,128)(2,1)S(1)} %collective-permute-done.7.refs_2_), channel_id=1, source_target_pairs={{0,1},{1,0},{2,3},{3,2},{4,5},{5,4},{6,7},{7,6},{8,9},{9,8},{10,11... | collective-permute-start | bytes 786440 | tf_op jit(solution)/shard_map/ppermute | solution.py:220
  43.3 8.9 %copy-start.5 = (bf16[256,1024]{1,0:T(8,128)(2,1)}, bf16[256,1024]{1,0:T(8,128)(2,1)S(1)}, u32[]{:S(2)}) copy-start(bf16[256,1024]{1,0:T(8,128)(2,1)S(1)} %collective-permute-done.refs_1_) | copy-start | bytes 1572868
  43.3 20.6 %collective-permute-start.10 = (bf16[512,384]{1,0:T(8,128)(2,1)S(1)}, bf16[512,384]{1,0:T(8,128)(2,1)}, u32[]{:S(2)}, u32[]{:S(2)}) collective-permute-start(bf16[512,384]{1,0:T(8,128)(2,1)S(1)} %pad_maximum_fusion.refs_5_), channel_id=1, source_target_pairs={{0,4},{2,6},{4,0},{6,2},{1,5},{3,7},{5,1},{7,3},{8,12},{10,14},{12... | collective-permute-start | bytes 1179656 | tf_op jit(solution)/shard_map/ppermute | solution.py:220
  44.9 9.9 %copy-start.6 = (bf16[256,1024]{1,0:T(8,128)(2,1)}, bf16[256,1024]{1,0:T(8,128)(2,1)S(1)}, u32[]{:S(2)}) copy-start(bf16[256,1024]{1,0:T(8,128)(2,1)S(1)} %collective-permute-done.2.refs_1_) | copy-start | bytes 1572868
  44.9 19.0 %collective-permute-start.11 = (bf16[512,384]{1,0:T(8,128)(2,1)S(1)}, bf16[512,384]{1,0:T(8,128)(2,1)}, u32[]{:S(2)}, u32[]{:S(2)}) collective-permute-start(bf16[512,384]{1,0:T(8,128)(2,1)S(1)} %pad_maximum_fusion.refs_5_), channel_id=1, source_target_pairs={{0,6},{2,4},{4,2},{6,0},{1,7},{3,5},{5,3},{7,1},{8,14},{10,12},{12... | collective-permute-start | bytes 1179656 | tf_op jit(solution)/shard_map/ppermute | solution.py:220
  46.4 33.8 %copy-start.2 = (bf16[512,384]{1,0:T(8,128)(2,1)}, bf16[512,384]{1,0:T(8,128)(2,1)S(1)}, u32[]{:S(2)}) copy-start(bf16[512,384]{1,0:T(8,128)(2,1)S(1)} %pad_maximum_fusion.1.refs_5_) | copy-start | bytes 1179652
  46.4 2.1 %copy-start.7 = (bf16[256,1024]{1,0:T(8,128)(2,1)}, bf16[256,1024]{1,0:T(8,128)(2,1)S(1)}, u32[]{:S(2)}) copy-start(bf16[256,1024]{1,0:T(8,128)(2,1)S(1)} %collective-permute-done.4.refs_3_) | copy-start | bytes 1572868
  46.4 29.9 %collective-permute-start.16 = (bf16[512,384]{1,0:T(8,128)(2,1)S(1)}, bf16[512,384]{1,0:T(8,128)(2,1)}, u32[]{:S(2)}, u32[]{:S(2)}) collective-permute-start(bf16[512,384]{1,0:T(8,128)(2,1)S(1)} %pad_maximum_fusion.1.refs_5_), channel_id=1, source_target_pairs={{0,2},{2,0},{4,6},{6,4},{1,3},{3,1},{5,7},{7,5},{8,10},{10,8},{12,... | collective-permute-start | bytes 1179656 | tf_op jit(solution)/shard_map/ppermute | solution.py:220
  47.0 1.5 %copy-start.11 = (bf16[128,1024]{1,0:T(8,128)(2,1)}, bf16[128,1024]{1,0:T(8,128)(2,1)S(1)}, u32[]{:S(2)}) copy-start(bf16[128,1024]{1,0:T(8,128)(2,1)S(1)} %collective-permute-done.6.refs_1_) | copy-start | bytes 786436
  47.0 33.2 %collective-permute-start.17 = (bf16[512,384]{1,0:T(8,128)(2,1)S(1)}, bf16[512,384]{1,0:T(8,128)(2,1)}, u32[]{:S(2)}, u32[]{:S(2)}) collective-permute-start(bf16[512,384]{1,0:T(8,128)(2,1)S(1)} %pad_maximum_fusion.1.refs_5_), channel_id=1, source_target_pairs={{0,4},{2,6},{4,0},{6,2},{1,5},{3,7},{5,1},{7,3},{8,12},{10,14},{12... | collective-permute-start | bytes 1179656 | tf_op jit(solution)/shard_map/ppermute | solution.py:220
  48.6 0.7 copy-start.12
  49.3 30.9 %collective-permute-start.18 = (bf16[512,384]{1,0:T(8,128)(2,1)S(1)}, bf16[512,384]{1,0:T(8,128)(2,1)}, u32[]{:S(2)}, u32[]{:S(2)}) collective-permute-start(bf16[512,384]{1,0:T(8,128)(2,1)S(1)} %pad_maximum_fusion.1.refs_5_), channel_id=1, source_target_pairs={{0,6},{2,4},{4,2},{6,0},{1,7},{3,5},{5,3},{7,1},{8,14},{10,12},{12... | collective-permute-start | bytes 1179656 | tf_op jit(solution)/shard_map/ppermute | solution.py:220
  72.9 17.4 %collective-permute-start.12 = (bf16[256,128]{1,0:T(8,128)(2,1)}, bf16[256,128]{1,0:T(8,128)(2,1)S(1)}, u32[]{:S(2)}, u32[]{:S(2)}) collective-permute-start(bf16[256,128]{1,0:T(8,128)(2,1)} %get-tuple-element.26), channel_id=1, source_target_pairs={{0,8},{8,16},{16,24},{24,0},{1,9},{9,17},{17,25},{25,1},{2,10},{10... | collective-permute-start | bytes 196616 | tf_op jit(solution)/shard_map/ppermute | solution.py:220
  74.2 17.4 %collective-permute-start.13 = (bf16[256,128]{1,0:T(8,128)(2,1)}, bf16[256,128]{1,0:T(8,128)(2,1)S(1)}, u32[]{:S(2)}, u32[]{:S(2)}) collective-permute-start(bf16[256,128]{1,0:T(8,128)(2,1)} %get-tuple-element.27), channel_id=1, source_target_pairs={{0,16},{8,24},{16,0},{24,8},{1,17},{9,25},{17,1},{25,9},{2,18},{10... | collective-permute-start | bytes 196616 | tf_op jit(solution)/shard_map/ppermute | solution.py:220
  76.3 15.3 %collective-permute-start.14 = (bf16[256,128]{1,0:T(8,128)(2,1)}, bf16[256,128]{1,0:T(8,128)(2,1)S(1)}, u32[]{:S(2)}, u32[]{:S(2)}) collective-permute-start(bf16[256,128]{1,0:T(8,128)(2,1)} %get-tuple-element.28), channel_id=1, source_target_pairs={{0,24},{8,0},{16,8},{24,16},{1,25},{9,1},{17,9},{25,17},{2,26},{10... | collective-permute-start | bytes 196616 | tf_op jit(solution)/shard_map/ppermute | solution.py:220
  87.3 7.0 %collective-permute-start.19 = (bf16[256,128]{1,0:T(8,128)(2,1)}, bf16[256,128]{1,0:T(8,128)(2,1)S(1)}, u32[]{:S(2)}, u32[]{:S(2)}) collective-permute-start(bf16[256,128]{1,0:T(8,128)(2,1)} %get-tuple-element.32), channel_id=1, source_target_pairs={{0,8},{8,16},{16,24},{24,0},{1,9},{9,17},{17,25},{25,1},{2,10},{10... | collective-permute-start | bytes 196616 | tf_op jit(solution)/shard_map/ppermute | solution.py:220
  88.5 7.3 %collective-permute-start.20 = (bf16[256,128]{1,0:T(8,128)(2,1)}, bf16[256,128]{1,0:T(8,128)(2,1)S(1)}, u32[]{:S(2)}, u32[]{:S(2)}) collective-permute-start(bf16[256,128]{1,0:T(8,128)(2,1)} %get-tuple-element.33), channel_id=1, source_target_pairs={{0,16},{8,24},{16,0},{24,8},{1,17},{9,25},{17,1},{25,9},{2,18},{10... | collective-permute-start | bytes 196616 | tf_op jit(solution)/shard_map/ppermute | solution.py:220
  90.3 1.3 %copy-start.15 = (bf16[256,128]{1,0:T(8,128)(2,1)}, bf16[256,128]{1,0:T(8,128)(2,1)S(1)}, u32[]{:S(2)}) copy-start(bf16[256,128]{1,0:T(8,128)(2,1)S(1)} %collective-permute-done.12.refs_1_) | copy-start | bytes 196612
  90.3 5.5 %collective-permute-start.21 = (bf16[256,128]{1,0:T(8,128)(2,1)}, bf16[256,128]{1,0:T(8,128)(2,1)S(1)}, u32[]{:S(2)}, u32[]{:S(2)}) collective-permute-start(bf16[256,128]{1,0:T(8,128)(2,1)} %get-tuple-element.34), channel_id=1, source_target_pairs={{0,24},{8,0},{16,8},{24,16},{1,25},{9,1},{17,9},{25,17},{2,26},{10... | collective-permute-start | bytes 196616 | tf_op jit(solution)/shard_map/ppermute | solution.py:220
  91.6 0.6 copy-start.16
  91.6 0.6 copy-start.17
  93.9 4.2 %collective-permute-start.15 = (bf16[128,512]{1,0:T(8,128)(2,1)}, bf16[128,512]{1,0:T(8,128)(2,1)S(1)}, u32[]{:S(2)}, u32[]{:S(2)}) collective-permute-start(bf16[128,512]{1,0:T(8,128)(2,1)} %get-tuple-element.30), channel_id=1, source_target_pairs={{0,1},{1,0},{2,3},{3,2},{4,5},{5,4},{6,7},{7,6},{8,9},{9,8},{10,11... | collective-permute-start | bytes 393224 | tf_op jit(solution)/shard_map/ppermute | solution.py:220
  94.2 1.6 %copy-start.18 = (bf16[256,128]{1,0:T(8,128)(2,1)}, bf16[256,128]{1,0:T(8,128)(2,1)S(1)}, u32[]{:S(2)}) copy-start(bf16[256,128]{1,0:T(8,128)(2,1)S(1)} %collective-permute-done.19.refs_1_) | copy-start | bytes 196612
  95.8 0.6 copy-start.19
  95.8 0.6 copy-start.20
  98.1 1.6 %collective-permute-start.22 = (bf16[128,512]{1,0:T(8,128)(2,1)}, bf16[128,512]{1,0:T(8,128)(2,1)S(1)}, u32[]{:S(2)}, u32[]{:S(2)}) collective-permute-start(bf16[128,512]{1,0:T(8,128)(2,1)} %get-tuple-element.36), channel_id=1, source_target_pairs={{0,1},{1,0},{2,3},{3,2},{4,5},{5,4},{6,7},{7,6},{8,9},{9,8},{10,11... | collective-permute-start | bytes 393224 | tf_op jit(solution)/shard_map/ppermute | solution.py:220
  98.1 1.6 %copy-start.13 = (bf16[128,512]{1,0:T(8,128)(2,1)}, bf16[128,512]{1,0:T(8,128)(2,1)S(1)}, u32[]{:S(2)}) copy-start(bf16[128,512]{1,0:T(8,128)(2,1)S(1)} %collective-permute-done.15.refs_1_) | copy-start | bytes 393220
  99.7 0.6 copy-start.14
